TPU v7x, 32 devices: a whole 2x2x4 slice. The times are simulated.
32 devices in a mesh: fs: 4 (over y, x), tp: 8 (over z, core).
Axes of the slice: x: 2, y: 2, z: 4, core: 2. Of those that a mesh axis runs over, the one named last changes fastest.
Arguments:
- tokens: bfloat16 [512, 4096], P('fs', 'tp'), may hold values from -6 to 6
- expert_ids: int32 [512, 8], P('fs'), may hold values from 0 to 63, all different within a row; in each aligned block of 128 rows (0 to 127, 128 to 255, ...) at most 32 rows name the same one
- affinity: float32 [512, 8], P('fs'), may hold values from 0.05 to 1
- norm_gain: float32 [4096], P('fs'), may hold values from 0.1 to 1.9
- gate_train: float32 [64, 512, 4096], P(None, 'tp', 'fs'), may hold values from -0.09375 to 0.09375
- up_train: float32 [64, 512, 4096], P(None, 'tp', 'fs'), may hold values from -0.09375 to 0.09375
- down_train: float32 [64, 512, 4096], P(None, 'fs', 'tp'), may hold values from -0.25 to 0.25
- shared_gate_train: float32 [512, 4096], P('tp', 'fs'), may hold values from -0.09375 to 0.09375
- shared_up_train: float32 [512, 4096], P('tp', 'fs'), may hold values from -0.09375 to 0.09375
- shared_down_train: float32 [512, 4096], P('fs', 'tp'), may hold values from -0.25 to 0.25
Outputs:
- mixed: bfloat16 [512, 4096], P('fs', 'tp')
- gate_serve: bfloat16 [64, 512, 4096], P('fs', 'tp')
- up_serve: bfloat16 [64, 512, 4096], P('fs', 'tp')
- down_serve: bfloat16 [64, 512, 4096], P('fs', None, 'tp')
- shared_gate_serve: bfloat16 [512, 4096], P('tp')
- shared_up_serve: bfloat16 [512, 4096], P('tp')
- shared_down_serve: bfloat16 [512, 4096], P(None, 'tp')
Inputs may be any that keep to these rules, and one draw needn't show every extreme that they name: `expert_ids`: each row names 8 different experts. In each aligned block of 128 rows (the tokens of one index of fs) no expert is named by more than 32 rows, a bound that some block reaches.
All inputs are finite; a program needn't handle non-finite values.
Results may differ from a plain program's by a relative error of at most 0.019.
Values may be sent and summed in bfloat16 or wider, within the bound.
No kernel may reach another device: no remote copies, remote signals or barrier semaphores. Data moves between devices by JAX's collectives and lax.ppermute only.
A program may use at most 192 MiB of HBM per device.

v0:
```python
import functools

import jax
import jax.numpy as jnp
from jax import lax
from jax.experimental import pallas as pl
from jax.experimental.pallas import tpu as pltpu
from jax.sharding import PartitionSpec as P


K = 8

norm_eps = 1e-06
routed_scale = 2.5

VMEM_LIMIT = 60 * 1024 * 1024
ANY = pl.BlockSpec(memory_space=pl.ANY)
VMEM = pl.BlockSpec(memory_space=pltpu.VMEM)
SMEM = pl.BlockSpec(memory_space=pltpu.SMEM)


def partner(i, s, n):
    if n & (n - 1) == 0:
        return i ^ s, i ^ s
    return (i + s) % n, (i + n - s) % n


def exchange(x, axis, n, s):
    return lax.ppermute(x, axis, [(i, partner(i, s, n)[0]) for i in range(n)])


def give_back(x, axis, n, s):
    return lax.ppermute(x, axis, [(i, partner(i, s, n)[1]) for i in range(n)])


def gather_z(x):
    parts = lax.axis_size("tp")
    half = parts // 2
    got = [x]
    for s in range(1, half):
        pairs = [(i, 2 * partner(i // 2, s, half)[0] + i % 2) for i in range(parts)]
        got.append(lax.ppermute(x, "tp", pairs))
    return got


def swap_core(pieces):
    parts = lax.axis_size("tp")
    return [lax.ppermute(x, "tp", [(i, i ^ 1) for i in range(parts)]) for x in pieces]


def gathered_from():
    me = lax.axis_index("tp")
    half = lax.axis_size("tp") // 2
    chips = [partner(me >> 1, s, half)[1] for s in range(half)]
    return [2 * z + core for core in (me & 1, 1 - (me & 1)) for z in chips]


def cuts(count):
    marks = [0] + [-(-count * num // 16) for num in (4, 10, 16)]
    return [(lo, hi - lo) for lo, hi in zip(marks, marks[1:]) if hi > lo]


def down_cuts(chunks):
    steps = [(c, *chunks[c]) for c in range(1, len(chunks))]
    lo, count = chunks[0]
    head = count // 2
    return steps + [(0, *part) for part in ((lo, head), (lo + head, count - head)) if part[1]]


TOKEN = jax.ShapeDtypeStruct((8, 128), jnp.float32)


def prep_gu_body(n, idx_ref, gain_ref, *refs):
    gates, ups, outs = refs[:n], refs[n : 2 * n], refs[2 * n + 1 : 3 * n + 1]
    refs[-1][...] = jnp.zeros(TOKEN.shape, TOKEN.dtype)
    gain = gain_ref[...]
    for s in range(n):
        outs[s][0, 0] = (gates[s][0] * gain).astype(jnp.bfloat16)
        outs[s][1, 0] = (ups[s][0] * gain).astype(jnp.bfloat16)


def prep_gu(gate, up, gain, base, lo, count, token):
    n = base.shape[0]
    _, hp, df = gate.shape
    block = lambda s: pl.BlockSpec((1, hp, df), lambda i, idx, s=s: (idx[s] + i, 0, 0))
    return pl.pallas_call(
        functools.partial(prep_gu_body, n),
        grid_spec=pltpu.PrefetchScalarGridSpec(
            num_scalar_prefetch=1,
            grid=(count,),
            in_specs=[pl.BlockSpec((1, df), lambda i, idx: (0, 0))]
            + [block(s) for s in range(n)] * 2
            + [ANY],
            out_specs=[pl.BlockSpec((2, 1, hp, df), lambda i, idx: (0, i, 0, 0))] * n
            + [pl.BlockSpec(TOKEN.shape, lambda i, idx: (0, 0))],
        ),
        out_shape=[jax.ShapeDtypeStruct((2, count, hp, df), jnp.bfloat16)] * n + [TOKEN],
        compiler_params=pltpu.CompilerParams(vmem_limit_bytes=VMEM_LIMIT),
    )(base + lo, gain, *([gate] * n), *([up] * n), token)


def prep_down_body(n, idx_ref, *refs):
    refs[-1][...] = jnp.zeros(TOKEN.shape, TOKEN.dtype)
    for s in range(n):
        refs[n + 1 + s][0] = refs[s][0].astype(jnp.bfloat16)


def prep_down(down, base, lo, count, token):
    n = base.shape[0]
    _, hf, dp = down.shape
    block = lambda s: pl.BlockSpec((1, hf, dp), lambda i, idx, s=s: (idx[s] + i, 0, 0))
    return pl.pallas_call(
        functools.partial(prep_down_body, n),
        grid_spec=pltpu.PrefetchScalarGridSpec(
            num_scalar_prefetch=1,
            grid=(count,),
            in_specs=[block(s) for s in range(n)] + [ANY],
            out_specs=[pl.BlockSpec((1, hf, dp), lambda i, idx: (i, 0, 0))] * n
            + [pl.BlockSpec(TOKEN.shape, lambda i, idx: (0, 0))],
        ),
        out_shape=[jax.ShapeDtypeStruct((count, hf, dp), jnp.bfloat16)] * n + [TOKEN],
        compiler_params=pltpu.CompilerParams(vmem_limit_bytes=VMEM_LIMIT),
    )(base + lo, *([down] * n), token)


def pack_body(n, *refs):
    own = refs[0].shape[0]
    for s in range(n):
        refs[-1][s * own : (s + 1) * own, :] = refs[s][...]


def pack(pieces, token):
    n = len(pieces)
    own, dp = pieces[0].shape
    return pl.pallas_call(
        functools.partial(pack_body, n),
        in_specs=[VMEM] * n + [ANY],
        out_specs=VMEM,
        out_shape=jax.ShapeDtypeStruct((n * own, dp), pieces[0].dtype),
        name="pack_tokens",
    )(*pieces, token)


def route_body(n, parts, n_local, me_ref, from_ref, *refs):
    gathered, tables, (x_ref, w_ref, inv_ref) = refs[:parts], refs[parts : parts + n], refs[parts + n :]
    own = tables[0].shape[1]
    hp = w_ref.shape[1] // n_local
    width = x_ref.shape[0] * x_ref.shape[2]
    for s in range(n):
        at = pl.ds(s * own, own)
        squares = 0.0
        for k in range(parts):
            narrow = gathered[k][at, :]
            x_ref[from_ref[k], at, :] = narrow
            wide = narrow.astype(jnp.float32)
            squares = squares + jnp.sum(wide * wide, axis=1, keepdims=True)
        inv_ref[at, :] = lax.rsqrt(squares / width + norm_eps)
        table = tables[s][...].T
        ids, affinity = table[:, :K].astype(jnp.int32), table[:, K:]
        weight = routed_scale * affinity / jnp.sum(affinity, axis=1, keepdims=True)
        for e in range(n_local):
            hit = ids == me_ref[0] * n_local + e
            here = jnp.sum(jnp.where(hit, weight, 0.0), axis=1, keepdims=True)
            w_ref[at, e * hp : (e + 1) * hp] = jnp.broadcast_to(here, (own, hp))


def route(me, source, gathered, tables, n_local, hp):
    n, parts = len(tables), len(gathered)
    rows, dp = gathered[0].shape
    return pl.pallas_call(
        functools.partial(route_body, n, parts, n_local),
        in_specs=[SMEM] * 2 + [VMEM] * (parts + n),
        out_specs=[VMEM] * 3,
        out_shape=[
            jax.ShapeDtypeStruct((parts, rows, dp), gathered[0].dtype),
            jax.ShapeDtypeStruct((rows, n_local * hp), jnp.float32),
            jax.ShapeDtypeStruct((rows, 1), jnp.float32),
        ],
        compiler_params=pltpu.CompilerParams(vmem_limit_bytes=VMEM_LIMIT),
        name="route",
    )(me, source, *gathered, *tables)


def shared_down_body(n, parts, me_ref, from_ref, *refs):
    gathered, (down_ref, acc_ref) = refs[:parts], refs[parts:]
    lanes = gathered[0].shape[1]
    share = parts // n
    hp = down_ref.shape[0] // share
    acc_ref[...] = jnp.zeros(acc_ref.shape, acc_ref.dtype)
    for k in range(parts):

        @pl.when(from_ref[k] // share == me_ref[0])
        def _(k=k):
            rows = pl.ds(pl.multiple_of((from_ref[k] % share) * hp, hp), hp)
            acc_ref[...] += jnp.dot(
                gathered[k][:, lanes - hp :], down_ref[rows, :], preferred_element_type=jnp.float32
            )


def shared_down_part(n, me, source, gathered, down):
    parts = len(gathered)
    return pl.pallas_call(
        functools.partial(shared_down_body, n, parts),
        in_specs=[SMEM] * 2 + [VMEM] * (parts + 1),
        out_specs=VMEM,
        out_shape=jax.ShapeDtypeStruct((gathered[0].shape[0], down.shape[1]), jnp.float32),
        compiler_params=pltpu.CompilerParams(vmem_limit_bytes=VMEM_LIMIT),
        name="shared_down",
    )(me, source, *gathered, down)


def stack_rows_body(n, blk_ref, *refs):
    own = refs[0].shape[0]
    for s in range(n):
        refs[-1][pl.ds(pl.multiple_of(blk_ref[s] * own, own), own), :] = refs[s][...]


def stack_rows(blk, pieces, token):
    n = len(pieces)
    own, dp = pieces[0].shape
    return pl.pallas_call(
        functools.partial(stack_rows_body, n),
        in_specs=[SMEM] + [VMEM] * n + [ANY],
        out_specs=VMEM,
        out_shape=jax.ShapeDtypeStruct((n * own, dp), pieces[0].dtype),
        name="stack_rows",
    )(blk, *pieces, token)


def gu_body(n, lo, count, shared, first, *refs):
    refs = list(refs)
    take = lambda k: [refs.pop(0) for _ in range(k)]
    (blk_ref, x_ref, inv_ref, w_ref) = take(4)
    pieces = take(n)
    shared_pieces = take(n) if shared else []
    take(1 if first else 2)
    gate_out, up_out = take(2)
    shared_out = take(2) if shared else []
    (a_ref,) = take(1)
    buf, acc_g, acc_u, in_sem, out_sem = refs
    tot = count + (1 if shared else 0)
    hp, df = buf.shape[-2:]
    dp = x_ref.shape[-1]
    ratio = df // dp
    incoming = []
    for s in range(n):
        here = [pltpu.make_async_copy(pieces[s], buf.at[s, :, pl.ds(0, count)], in_sem.at[s, 0])]
        if shared:
            here.append(
                pltpu.make_async_copy(shared_pieces[s], buf.at[s, :, count], in_sem.at[s, 1])
            )
        for copy in here:
            copy.start()
        incoming.append(here)
    outgoing = []
    nt = (((1,), (1,)), ((), ()))
    for s in range(n):
        for copy in incoming[s]:
            copy.wait()
        blk = blk_ref[s]
        cols = pl.ds(pl.multiple_of(blk * df, df), df)
        here = []
        for m, out in enumerate((gate_out, up_out)):
            here.append(
                pltpu.make_async_copy(
                    buf.at[s, m, pl.ds(0, count)],
                    out.at[pl.ds(lo, count), :, cols],
                    out_sem.at[s, m, 0],
                )
            )
        for m, out in enumerate(shared_out):
            here.append(
                pltpu.make_async_copy(buf.at[s, m, count], out.at[:, cols], out_sem.at[s, m, 1])
            )
        for copy in here:
            copy.start()
        outgoing += here
        for m, acc in enumerate((acc_g, acc_u)):
            part = None
            for j in range(ratio):
                w = buf[s, m, :, :, j * dp : (j + 1) * dp].reshape(tot * hp, dp)
                dot = lax.dot_general(
                    x_ref[blk * ratio + j], w, nt, preferred_element_type=jnp.float32
                )
                part = dot if part is None else part + dot
            if s == 0:
                acc[...] = part
            else:
                acc[...] += part
    inv = inv_ref[...]
    routed = count * hp
    for lanes in [slice(0, routed)] + ([slice(routed, routed + hp)] if shared else []):
        gate = acc_g[:, lanes] * inv
        up = acc_u[:, lanes] * inv
        hidden = gate * jax.nn.sigmoid(gate) * up
        if lanes.start == 0:
            w = w_ref[:, lo * hp : lo * hp + routed]
            hidden = jnp.where(w > 0, hidden * w, 0.0)
        a_ref[:, lanes] = hidden.astype(jnp.bfloat16)
    for copy in outgoing:
        copy.wait()


def gu_step(blk, x, inv, w, pieces, shared_pieces, prev, token, lo, count, n_local, width):
    n = len(pieces)
    hp, df = pieces[0].shape[-2:]
    rows = x.shape[1]
    shared = bool(shared_pieces)
    tot = count + (1 if shared else 0)
    bf = jnp.bfloat16
    out_shape = [jax.ShapeDtypeStruct((n_local, hp, width), bf)] * 2
    if shared:
        out_shape += [jax.ShapeDtypeStruct((hp, width), bf)] * 2
    out_shape.append(jax.ShapeDtypeStruct((rows, tot * hp), bf))
    args = [blk, x, inv, w, *pieces, *shared_pieces, *(prev or [token])]
    specs = [SMEM, VMEM, VMEM, VMEM] + [ANY] * (len(args) - 4)
    aliases = {len(args) - 2: 0, len(args) - 1: 1} if prev else {}
    return pl.pallas_call(
        functools.partial(gu_body, n, lo, count, shared, not prev),
        in_specs=specs,
        out_specs=[ANY] * (len(out_shape) - 1) + [VMEM],
        out_shape=out_shape,
        scratch_shapes=[
            pltpu.VMEM((n, 2, tot, hp, df), bf),
            pltpu.VMEM((rows, tot * hp), jnp.float32),
            pltpu.VMEM((rows, tot * hp), jnp.float32),
            pltpu.SemaphoreType.DMA((n, 2)),
            pltpu.SemaphoreType.DMA((n, 2, 2)),
        ],
        input_output_aliases=aliases,
        compiler_params=pltpu.CompilerParams(vmem_limit_bytes=VMEM_LIMIT),
    )(*args)


def down_body(n, parts, lo, count, skip, first, last, *refs):
    refs = list(refs)
    take = lambda k: [refs.pop(0) for _ in range(k)]
    from_ref, blk_ref = take(2)
    gathered = take(parts)
    (acc_in,) = take(1)
    pieces = take(n)
    if not first:
        take(1)
    (down_out,) = take(1)
    results = take(n) if last else take(1)
    buf, in_sem, out_sem = refs
    hf = pieces[0].shape[1]
    copies = []
    for s in range(n):
        rows = pl.ds(pl.multiple_of(blk_ref[s] * hf, hf), hf)
        copies.append(pltpu.make_async_copy(pieces[s], buf.at[:, rows], in_sem.at[s]))
    for copy in copies:
        copy.start()
    for copy in copies:
        copy.wait()
    out = pltpu.make_async_copy(buf, down_out.at[pl.ds(lo, count)], out_sem)
    out.start()
    hp = buf.shape[1] // parts
    dp = buf.shape[2]
    lanes = slice(skip * hp, (skip + count) * hp)
    own = acc_in.shape[0] // n
    for r in range(n):
        at = pl.ds(r * own, own)
        total = acc_in[at, :]
        for k in range(parts):
            hidden = pl.ds(pl.multiple_of(from_ref[k] * hp, hp), hp)
            w = buf[:, hidden, :].reshape(count * hp, dp)
            total += jnp.dot(gathered[k][at, lanes], w, preferred_element_type=jnp.float32)
        if last:
            results[r][...] = total.astype(results[r].dtype)
        else:
            results[0][at, :] = total
    out.wait()


def down_step(source, blk, gathered, acc, pieces, prev, lo, count, skip, n_local, last):
    n, parts = len(pieces), len(gathered)
    _, hf, dp = pieces[0].shape
    rows = acc.shape[0]
    own = rows // n
    hidden = hf * n
    first = prev is None
    bf = jnp.bfloat16
    out_shape = [jax.ShapeDtypeStruct((n_local, hidden, dp), bf)]
    if last:
        out_shape.append(jax.ShapeDtypeStruct((own, dp), jnp.float32))
        out_shape += [jax.ShapeDtypeStruct((own, dp), bf)] * (n - 1)
    else:
        out_shape.append(jax.ShapeDtypeStruct((rows, dp), jnp.float32))
    args = [source, blk, *gathered, acc, *pieces] + ([] if first else [prev])
    return pl.pallas_call(
        functools.partial(down_body, n, parts, lo, count, skip, first, last),
        in_specs=[SMEM] * 2 + [VMEM] * (parts + 1) + [ANY] * (len(args) - parts - 3),
        out_specs=[ANY] + [VMEM] * (len(out_shape) - 1),
        out_shape=out_shape,
        scratch_shapes=[
            pltpu.VMEM((count, hidden, dp), bf),
            pltpu.SemaphoreType.DMA((n,)),
            pltpu.SemaphoreType.DMA,
        ],
        input_output_aliases={} if first else {len(args) - 1: 0},
        compiler_params=pltpu.CompilerParams(vmem_limit_bytes=VMEM_LIMIT),
    )(*args)


def layer(
    n,
    tokens,
    expert_ids,
    affinity,
    norm_gain,
    gate_train,
    up_train,
    down_train,
    shared_gate_train,
    shared_up_train,
    shared_down_train,
):
    bf = jnp.bfloat16
    me = lax.axis_index("fs")
    experts, hp, _ = gate_train.shape
    n_local = experts // n
    width = norm_gain.shape[0] * n
    to = [partner(me, s, n)[0] for s in range(n)]
    blk = jnp.stack([partner(me, s, n)[1] for s in range(n)]).astype(jnp.int32)
    base = (jnp.stack(to) * n_local).astype(jnp.int32)
    gain = norm_gain[None, :]

    def swap(pieces):
        return [pieces[0]] + [exchange(pieces[s], "fs", n, s) for s in range(1, n)]

    token_pieces = swap([tokens] * n)

    shared_gu = (jnp.stack([shared_gate_train, shared_up_train]) * gain).astype(bf)
    shared_gu = swap([shared_gu] * n)
    table = jnp.concatenate([expert_ids.astype(jnp.float32).T, affinity.T])
    tables = swap([table] * n)
    chunks = cuts(n_local)
    steps = down_cuts(chunks)
    token = jnp.zeros(TOKEN.shape, TOKEN.dtype)
    gu, down = {}, {}
    for c, (lo, count) in enumerate(chunks):
        *pieces, token = prep_gu(gate_train, up_train, gain, base, lo, count, token)
        gu[c] = swap(pieces)
        if c == 0:
            token = packed = pack(token_pieces, token)
            x_same = gather_z(packed)
    for i, (_, lo, count) in enumerate(steps):
        *pieces, token = prep_down(down_train, base, lo, count, token)
        down[i] = swap(pieces)
    own_shared_down = shared_down_train.astype(bf)
    shared_down = swap([own_shared_down] * n)

    x_all = x_same + swap_core(x_same)
    me = me.astype(jnp.int32)[None]
    source = jnp.stack(gathered_from()).astype(jnp.int32)
    x, w, inv = route(me, source, x_all, tables, n_local, hp)
    prev, gathered = [], []
    for c, (lo, count) in enumerate(chunks):
        results = gu_step(
            *(blk, x, inv, w, gu[c], shared_gu if c == 0 else []),
            *(prev, token, lo, count, n_local, width),
        )
        if c == 0:
            shared_gate_serve, shared_up_serve = results[2:4]
        prev = results[:2]
        same = gather_z(results[-1])
        gathered.append(same + swap_core(same))
    gate_serve, up_serve = prev

    acc = shared_down_part(n, me, source, gathered[0], own_shared_down)
    down_serve = None
    for i, (c, lo, count) in enumerate(steps):
        last = i == len(steps) - 1
        skip = lo - chunks[c][0]
        down_serve, acc, *sums = down_step(
            *(source, blk, gathered[c], acc, down[i], down_serve),
            *(lo, count, skip, n_local, last),
        )
    shared_down_serve = stack_rows(blk, shared_down, acc)
    sums = [acc, *sums]
    total = sums[0]
    for s in range(1, n):
        total = total + give_back(sums[s], "fs", n, s).astype(jnp.float32)
    return (
        total.astype(bf),
        gate_serve,
        up_serve,
        down_serve,
        shared_gate_serve,
        shared_up_serve,
        shared_down_serve,
    )


def body(n, *args):
    return layer(n, *args)


def solution(mesh):
    n = mesh.shape["fs"]
    return jax.shard_map(
        functools.partial(body, n),
        mesh=mesh,
        in_specs=(
            P("fs", "tp"),
            P("fs", None),
            P("fs", None),
            P("fs"),
            P(None, "tp", "fs"),
            P(None, "tp", "fs"),
            P(None, "fs", "tp"),
            P("tp", "fs"),
            P("tp", "fs"),
            P("fs", "tp"),
        ),
        out_specs=(
            P("fs", "tp"),
            P("fs", "tp", None),
            P("fs", "tp", None),
            P("fs", None, "tp"),
            P("tp", None),
            P("tp", None),
            P(None, "tp"),
        ),
        check_vma=False,
    )
```

profile of v0, /device:TPU:0, one launch (start us, length us, event | category | flops | bytes accessed | tf_op | source)
XLA Modules:
  0.0 512.0 jit_solution(4380414246155811004)
XLA Ops:
  13.9 6.4 %shard_map.153 = (bf16[2,4,64,1024]{3,2,1,0:T(8,128)(2,1)}, bf16[2,4,64,1024]{3,2,1,0:T(8,128)(2,1)}, bf16[2,4,64,1024]{3,2,1,0:T(8,128)(2,1)}, bf16[2,4,64,1024]{3,2,1,0:T(8,128)(2,1)}, f32[8,128]{1,0:T(8,128)}) custom-call(s32[4]{0:T(128)} %get-tuple-element.131.idx_ref, f32[1,1024]{1,0:T(1,128)} %bitcast.20, f32[64,64,1024]{2,1,0:T(8,128)} %refs_3_.9, ...), custom_call_target="tpu_custom_call" | custom-call | tf_op jit(solution)/shard_map/pallas_call | solution.py:86
  23.2 8.9 %shard_map.154 = (bf16[2,6,64,1024]{3,2,1,0:T(8,128)(2,1)}, bf16[2,6,64,1024]{3,2,1,0:T(8,128)(2,1)}, bf16[2,6,64,1024]{3,2,1,0:T(8,128)(2,1)}, bf16[2,6,64,1024]{3,2,1,0:T(8,128)(2,1)}, f32[8,128]{1,0:T(8,128)}) custom-call(s32[4]{0:T(128)} %get-tuple-element.127.idx_ref, f32[1,1024]{1,0:T(1,128)} %bitcast.21, f32[64,64,1024]{2,1,0:T(8,128)} %refs_3_.9, ...), custom_call_target="tpu_custom_call" | custom-call | tf_op jit(solution)/shard_map/pallas_call | solution.py:86
  32.1 8.9 %shard_map.155 = (bf16[2,6,64,1024]{3,2,1,0:T(8,128)(2,1)}, bf16[2,6,64,1024]{3,2,1,0:T(8,128)(2,1)}, bf16[2,6,64,1024]{3,2,1,0:T(8,128)(2,1)}, bf16[2,6,64,1024]{3,2,1,0:T(8,128)(2,1)}, f32[8,128]{1,0:T(8,128)}) custom-call(s32[4]{0:T(128)} %get-tuple-element.129.idx_ref, f32[1,1024]{1,0:T(1,128)} %bitcast.22, f32[64,64,1024]{2,1,0:T(8,128)} %refs_3_.9, ...), custom_call_target="tpu_custom_call" | custom-call | tf_op jit(solution)/shard_map/pallas_call | solution.py:86
  41.0 6.5 %shard_map.156 = (bf16[6,128,512]{2,1,0:T(8,128)(2,1)}, bf16[6,128,512]{2,1,0:T(8,128)(2,1)}, bf16[6,128,512]{2,1,0:T(8,128)(2,1)}, bf16[6,128,512]{2,1,0:T(8,128)(2,1)}, f32[8,128]{1,0:T(8,128)}) custom-call(s32[4]{0:T(128)} %get-tuple-element.127.idx_ref, f32[64,128,512]{2,1,0:T(8,128)} %refs_3_.13, f32[64,128,512]{2,1,0:T(8,128)} %refs_3_.13, ...), custom_call_target="tpu_custom_call" | custom-call | tf_op jit(solution)/shard_map/pallas_call | solution.py:112
  47.5 6.5 %shard_map.157 = (bf16[6,128,512]{2,1,0:T(8,128)(2,1)}, bf16[6,128,512]{2,1,0:T(8,128)(2,1)}, bf16[6,128,512]{2,1,0:T(8,128)(2,1)}, bf16[6,128,512]{2,1,0:T(8,128)(2,1)}, f32[8,128]{1,0:T(8,128)}) custom-call(s32[4]{0:T(128)} %get-tuple-element.129.idx_ref, f32[64,128,512]{2,1,0:T(8,128)} %refs_3_.13, f32[64,128,512]{2,1,0:T(8,128)} %refs_3_.13, ...), custom_call_target="tpu_custom_call" | custom-call | tf_op jit(solution)/shard_map/pallas_call | solution.py:112
  60.8 4.6 collective-permute-done.12.refs_11_
  72.8 3.7 collective-permute-start.5
  77.7 7.7 %collective-permute-done.53.refs_13_ = bf16[2,128,512]{2,1,0:T(8,128)(2,1)S(1)} collective-permute-done((bf16[2,128,512]{2,1,0:T(8,128)(2,1)}, bf16[2,128,512]{2,1,0:T(8,128)(2,1)S(1)}, u32[]{:S(2)}, u32[]{:S(2)}) %collective-permute-start.53) | collective-permute-done | bytes 262176 | tf_op jit(solution)/shard_map/ppermute | solution.py:29
  90.0 31.8 %collective-permute-done.4.refs_2_ = bf16[512,512]{1,0:T(8,128)(2,1)S(1)} collective-permute-done((bf16[512,512]{1,0:T(8,128)(2,1)S(1)}, bf16[512,512]{1,0:T(8,128)(2,1)S(1)}, u32[]{:S(2)}, u32[]{:S(2)}) %collective-permute-start.4) | collective-permute-done | bytes 524320 | tf_op jit(solution)/shard_map/ppermute | solution.py:42
  129.0 40.2 %collective-permute-done.14.refs_6_ = bf16[2,4,64,1024]{3,2,1,0:T(8,128)(2,1)S(1)} collective-permute-done((bf16[2,4,64,1024]{3,2,1,0:T(8,128)(2,1)}, bf16[2,4,64,1024]{3,2,1,0:T(8,128)(2,1)S(1)}, u32[]{:S(2)}, u32[]{:S(2)}) %collective-permute-start.14) | collective-permute-done | bytes 1048608 | tf_op jit(solution)/shard_map/ppermute | solution.py:29
  179.2 7.4 %route.1 = (bf16[8,512,512]{2,1,0:T(8,128)(2,1)}, f32[512,1024]{1,0:T(8,128)}, f32[512,1]{1,0:T(8,128)}) custom-call(s32[1]{0:T(128)} %bitcast.8.me_ref, s32[8]{0:T(128)} %stack.64.from_ref.refs_0_, bf16[512,512]{1,0:T(8,128)(2,1)} %pack_tokens.1.refs_0_.refs_8_, bf16[512,512]{1,0:T(8,128)(2,1)} %copy-done.22, bf16[512,512]{1,0:T(8,128)(2,1)} %copy-done.21, ...), custom_call_target="tpu_custom_call" | custom-call | tf_op jit(solution)/shard_map/route/pallas_call | solution.py:170
  186.6 10.3 %shard_map.160 = (bf16[16,64,4096]{2,1,0:T(8,128)(2,1)}, bf16[16,64,4096]{2,1,0:T(8,128)(2,1)}, bf16[64,4096]{1,0:T(8,128)(2,1)}, bf16[64,4096]{1,0:T(8,128)(2,1)}, bf16[512,320]{1,0:T(8,128)(2,1)}) custom-call(s32[4]{0:T(128)} %copy-done.50, bf16[8,512,512]{2,1,0:T(8,128)(2,1)} %get-tuple-element.68.refs_1_, f32[512,1]{1,0:T(8,128)} %get-tuple-element.69.refs_2_, ...), custom_call_target="tpu_custom_call" | custom-call | tf_op jit(solution)/shard_map/pallas_call | solution.py:318
  196.9 3.7 collective-permute-done.48.refs_14_
  200.7 4.0 collective-permute-start.21
  204.7 11.8 %collective-permute-done.49.refs_12_ = bf16[6,128,512]{2,1,0:T(8,128)(2,1)} collective-permute-done((bf16[6,128,512]{2,1,0:T(8,128)(2,1)}, bf16[6,128,512]{2,1,0:T(8,128)(2,1)}, u32[]{:S(2)}, u32[]{:S(2)}) %collective-permute-start.49) | collective-permute-done | bytes 786464 | tf_op jit(solution)/shard_map/ppermute | solution.py:29
  216.5 4.2 collective-permute-start.20
  222.2 14.8 %collective-permute-done.20.refs_2_.refs_4_ = bf16[512,320]{1,0:T(8,128)(2,1)S(1)} collective-permute-done((bf16[512,320]{1,0:T(8,128)(2,1)}, bf16[512,320]{1,0:T(8,128)(2,1)S(1)}, u32[]{:S(2)}, u32[]{:S(2)}) %collective-permute-start.20) | collective-permute-done | bytes 327712 | tf_op jit(solution)/shard_map/ppermute | solution.py:42
  240.0 36.2 %collective-permute-done.30.refs_6_ = bf16[2,6,64,1024]{3,2,1,0:T(8,128)(2,1)S(1)} collective-permute-done((bf16[2,6,64,1024]{3,2,1,0:T(8,128)(2,1)}, bf16[2,6,64,1024]{3,2,1,0:T(8,128)(2,1)S(1)}, u32[]{:S(2)}, u32[]{:S(2)}) %collective-permute-start.30) | collective-permute-done | bytes 1572896 | tf_op jit(solution)/shard_map/ppermute | solution.py:29
  278.7 12.6 %collective-permute-done.26.refs_5_ = bf16[2,6,64,1024]{3,2,1,0:T(8,128)(2,1)S(1)} collective-permute-done((bf16[2,6,64,1024]{3,2,1,0:T(8,128)(2,1)}, bf16[2,6,64,1024]{3,2,1,0:T(8,128)(2,1)S(1)}, u32[]{:S(2)}, u32[]{:S(2)}) %collective-permute-start.26) | collective-permute-done | bytes 1572896 | tf_op jit(solution)/shard_map/ppermute | solution.py:29
  291.5 68.4 %collective-permute-done.27.refs_6_ = bf16[2,6,64,1024]{3,2,1,0:T(8,128)(2,1)S(1)} collective-permute-done((bf16[2,6,64,1024]{3,2,1,0:T(8,128)(2,1)}, bf16[2,6,64,1024]{3,2,1,0:T(8,128)(2,1)S(1)}, u32[]{:S(2)}, u32[]{:S(2)}) %collective-permute-start.27) | collective-permute-done | bytes 1572896 | tf_op jit(solution)/shard_map/ppermute | solution.py:29
  361.6 10.1 %shard_map.161 = (bf16[16,64,4096]{2,1,0:T(8,128)(2,1)}, bf16[16,64,4096]{2,1,0:T(8,128)(2,1)}, bf16[512,384]{1,0:T(8,128)(2,1)}) custom-call(s32[4]{0:T(128)} %copy-done.50, bf16[8,512,512]{2,1,0:T(8,128)(2,1)} %get-tuple-element.68.refs_1_, f32[512,1]{1,0:T(8,128)} %get-tuple-element.69.refs_2_, ...), custom_call_target="tpu_custom_call", output_to_operand_aliasing={{0}: (8, {}), {1}: (9, {})} | custom-call | tf_op jit(solution)/shard_map/pallas_call | solution.py:318
  371.7 10.3 %shard_map.162 = (bf16[16,64,4096]{2,1,0:T(8,128)(2,1)}, bf16[16,64,4096]{2,1,0:T(8,128)(2,1)}, bf16[512,384]{1,0:T(8,128)(2,1)}) custom-call(s32[4]{0:T(128)} %copy-done.50, bf16[8,512,512]{2,1,0:T(8,128)(2,1)} %get-tuple-element.68.refs_1_, f32[512,1]{1,0:T(8,128)} %get-tuple-element.69.refs_2_, ...), custom_call_target="tpu_custom_call", output_to_operand_aliasing={{0}: (8, {}), {1}: (9, {})} | custom-call | tf_op jit(solution)/shard_map/pallas_call | solution.py:318
  384.7 3.4 collective-permute-start.33
  392.6 3.8 collective-permute-done.34.refs_5_
  396.4 18.3 %collective-permute-start.40 = (bf16[512,384]{1,0:T(8,128)(2,1)S(1)}, bf16[512,384]{1,0:T(8,128)(2,1)S(1)}, u32[]{:S(2)}, u32[]{:S(2)}) collective-permute-start(bf16[512,384]{1,0:T(8,128)(2,1)S(1)} %copy-done.26), channel_id=1, source_target_pairs={{0,4},{1,5},{2,6},{3,7},{4,0},{5,1},{6,2},{7,3},{8,12},{9,13},{10,... | collective-permute-start | bytes 1179656 | tf_op jit(solution)/shard_map/ppermute | solution.py:42
  414.7 23.2 %collective-permute-done.33.refs_4_ = bf16[512,384]{1,0:T(8,128)(2,1)S(1)} collective-permute-done((bf16[512,384]{1,0:T(8,128)(2,1)}, bf16[512,384]{1,0:T(8,128)(2,1)S(1)}, u32[]{:S(2)}, u32[]{:S(2)}) %collective-permute-start.33) | collective-permute-done | bytes 393248 | tf_op jit(solution)/shard_map/ppermute | solution.py:42
  438.6 16.2 %collective-permute-done.40.refs_4_ = bf16[512,384]{1,0:T(8,128)(2,1)S(1)} collective-permute-done((bf16[512,384]{1,0:T(8,128)(2,1)S(1)}, bf16[512,384]{1,0:T(8,128)(2,1)S(1)}, u32[]{:S(2)}, u32[]{:S(2)}) %collective-permute-start.40) | collective-permute-done | bytes 393248 | tf_op jit(solution)/shard_map/ppermute | solution.py:42
  467.0 3.6 shared_down.1.refs_10_
  470.6 8.6 %shard_map.163 = (bf16[16,512,512]{2,1,0:T(8,128)(2,1)}, f32[512,512]{1,0:T(8,128)}) custom-call(s32[8]{0:T(128)} %stack.64.from_ref.refs_0_, s32[4]{0:T(128)} %copy-done.50, bf16[512,384]{1,0:T(8,128)(2,1)} %get-tuple-element.95.refs_2_, bf16[512,384]{1,0:T(8,128)(2,1)} %copy-done.36, bf16[512,384]{1,0:T(8,128)(2,1)} %copy-done.34, ...), custom_call_target="tpu_custom_call" | custom-call | tf_op jit(solution)/shard_map/pallas_call | solution.py:391
  479.2 8.6 %shard_map.164 = (bf16[16,512,512]{2,1,0:T(8,128)(2,1)}, f32[512,512]{1,0:T(8,128)}) custom-call(s32[8]{0:T(128)} %stack.64.from_ref.refs_0_, s32[4]{0:T(128)} %copy-done.50, bf16[512,384]{1,0:T(8,128)(2,1)} %get-tuple-element.94.refs_2_, bf16[512,384]{1,0:T(8,128)(2,1)} %copy-done.30, ...), custom_call_target="tpu_custom_call", output_to_operand_aliasing={{0}: (15, {})} | custom-call | tf_op jit(solution)/shard_map/pallas_call | solution.py:391
  489.3 6.2 %shard_map.165 = (bf16[16,512,512]{2,1,0:T(8,128)(2,1)}, f32[512,512]{1,0:T(8,128)}) custom-call(s32[8]{0:T(128)} %stack.64.from_ref.refs_0_, s32[4]{0:T(128)} %copy-done.50, bf16[512,320]{1,0:T(8,128)(2,1)} %get-tuple-element.81.refs_0_.refs_2_, bf16[512,320]{1,0:T(8,128)(2,1)} %copy-done.4, ...), custom_call_target="tpu_custom_call", output_to_operand_aliasing={{0}: (15, {})} | custom-call | tf_op jit(solution)/shard_map/pallas_call | solution.py:391
  497.1 6.0 %shard_map.166 = (bf16[16,512,512]{2,1,0:T(8,128)(2,1)}, f32[128,512]{1,0:T(8,128)}, bf16[128,512]{1,0:T(8,128)(2,1)}, bf16[128,512]{1,0:T(8,128)(2,1)}, bf16[128,512]{1,0:T(8,128)(2,1)}) custom-call(s32[8]{0:T(128)} %stack.64.from_ref.refs_0_, s32[4]{0:T(128)} %copy-done.50, ...), custom_call_target="tpu_custom_call", output_to_operand_aliasing={{0}: (15, {})} | custom-call | tf_op jit(solution)/shard_map/pallas_call | solution.py:391
  (241 shorter events, 93.9 us)
Async XLA Ops:
  7.0 65.8 %collective-permute-start.18 = (bf16[2,64,1024]{2,1,0:T(8,128)(2,1)}, bf16[2,64,1024]{2,1,0:T(8,128)(2,1)}, u32[]{:S(2)}, u32[]{:S(2)}) collective-permute-start(bf16[2,64,1024]{2,1,0:T(8,128)(2,1)} %fusion.refs_8_), channel_id=1, source_target_pairs={{0,24},{8,16},{16,8},{24,0},{1,25},{9,17},{17,9},{25,1},{2,26},{10... | collective-permute-start | bytes 786440 | tf_op jit(solution)/shard_map/ppermute | solution.py:29
  9.9 66.6 %collective-permute-start.17 = (bf16[2,64,1024]{2,1,0:T(8,128)(2,1)}, bf16[2,64,1024]{2,1,0:T(8,128)(2,1)}, u32[]{:S(2)}, u32[]{:S(2)}) collective-permute-start(bf16[2,64,1024]{2,1,0:T(8,128)(2,1)} %fusion.refs_8_), channel_id=1, source_target_pairs={{0,16},{8,24},{16,0},{24,8},{1,17},{9,25},{17,1},{25,9},{2,18},{10... | collective-permute-start | bytes 786440 | tf_op jit(solution)/shard_map/ppermute | solution.py:29
  20.4 56.1 %collective-permute-start.16 = (bf16[2,64,1024]{2,1,0:T(8,128)(2,1)}, bf16[2,64,1024]{2,1,0:T(8,128)(2,1)S(1)}, u32[]{:S(2)}, u32[]{:S(2)}) collective-permute-start(bf16[2,64,1024]{2,1,0:T(8,128)(2,1)} %fusion.refs_8_), channel_id=1, source_target_pairs={{0,8},{8,0},{16,24},{24,16},{1,9},{9,1},{17,25},{25,17},{2,10},{10... | collective-permute-start | bytes 786440 | tf_op jit(solution)/shard_map/ppermute | solution.py:29
  76.4 45.4 %collective-permute-start.4 = (bf16[512,512]{1,0:T(8,128)(2,1)S(1)}, bf16[512,512]{1,0:T(8,128)(2,1)S(1)}, u32[]{:S(2)}, u32[]{:S(2)}) collective-permute-start(bf16[512,512]{1,0:T(8,128)(2,1)S(1)} %copy-done), channel_id=1, source_target_pairs={{0,4},{1,5},{2,6},{3,7},{4,0},{5,1},{6,2},{7,3},{8,12},{9,13},{10,... | collective-permute-start | bytes 1572872 | tf_op jit(solution)/shard_map/ppermute | solution.py:42
  76.5 45.9 %collective-permute-start.3 = (bf16[512,512]{1,0:T(8,128)(2,1)S(1)}, bf16[512,512]{1,0:T(8,128)(2,1)S(1)}, u32[]{:S(2)}, u32[]{:S(2)}) collective-permute-start(bf16[512,512]{1,0:T(8,128)(2,1)S(1)} %copy-done), channel_id=1, source_target_pairs={{0,2},{1,3},{2,0},{3,1},{4,6},{5,7},{6,4},{7,5},{8,10},{9,11},{10,... | collective-permute-start | bytes 1572872 | tf_op jit(solution)/shard_map/ppermute | solution.py:42
  85.4 43.5 %collective-permute-start.13 = (bf16[2,4,64,1024]{3,2,1,0:T(8,128)(2,1)}, bf16[2,4,64,1024]{3,2,1,0:T(8,128)(2,1)S(1)}, u32[]{:S(2)}, u32[]{:S(2)}) collective-permute-start(bf16[2,4,64,1024]{3,2,1,0:T(8,128)(2,1)} %get-tuple-element.72), channel_id=1, source_target_pairs={{0,8},{8,0},{16,24},{24,16},{1,9},{9,1},{17,25},{25,17},{2,10},{10... | collective-permute-start | bytes 3145736 | tf_op jit(solution)/shard_map/ppermute | solution.py:29
  86.9 40.4 %collective-permute-start.46 = (bf16[6,128,512]{2,1,0:T(8,128)(2,1)S(1)}, bf16[6,128,512]{2,1,0:T(8,128)(2,1)S(1)}, u32[]{:S(2)}, u32[]{:S(2)}) collective-permute-start(bf16[6,128,512]{2,1,0:T(8,128)(2,1)S(1)} %copy-done.58), channel_id=1, source_target_pairs={{0,8},{8,0},{16,24},{24,16},{1,9},{9,1},{17,25},{25,17},{2,10},{10... | collective-permute-start | bytes 2359304 | tf_op jit(solution)/shard_map/ppermute | solution.py:29
  89.6 37.7 %collective-permute-start.47 = (bf16[6,128,512]{2,1,0:T(8,128)(2,1)S(1)}, bf16[6,128,512]{2,1,0:T(8,128)(2,1)S(1)}, u32[]{:S(2)}, u32[]{:S(2)}) collective-permute-start(bf16[6,128,512]{2,1,0:T(8,128)(2,1)S(1)} %copy-done.57), channel_id=1, source_target_pairs={{0,16},{8,24},{16,0},{24,8},{1,17},{9,25},{17,1},{25,9},{2,18},{10... | collective-permute-start | bytes 2359304 | tf_op jit(solution)/shard_map/ppermute | solution.py:29
  121.8 47.4 %collective-permute-start.14 = (bf16[2,4,64,1024]{3,2,1,0:T(8,128)(2,1)}, bf16[2,4,64,1024]{3,2,1,0:T(8,128)(2,1)S(1)}, u32[]{:S(2)}, u32[]{:S(2)}) collective-permute-start(bf16[2,4,64,1024]{3,2,1,0:T(8,128)(2,1)} %get-tuple-element.73), channel_id=1, source_target_pairs={{0,16},{8,24},{16,0},{24,8},{1,17},{9,25},{17,1},{25,9},{2,18},{10... | collective-permute-start | bytes 3145736 | tf_op jit(solution)/shard_map/ppermute | solution.py:29
  122.4 48.3 %collective-permute-start.15 = (bf16[2,4,64,1024]{3,2,1,0:T(8,128)(2,1)}, bf16[2,4,64,1024]{3,2,1,0:T(8,128)(2,1)S(1)}, u32[]{:S(2)}, u32[]{:S(2)}) collective-permute-start(bf16[2,4,64,1024]{3,2,1,0:T(8,128)(2,1)} %get-tuple-element.74), channel_id=1, source_target_pairs={{0,24},{8,16},{16,8},{24,0},{1,25},{9,17},{17,9},{25,1},{2,26},{10... | collective-permute-start | bytes 3145736 | tf_op jit(solution)/shard_map/ppermute | solution.py:29
  127.3 43.9 %collective-permute-start.9 = (bf16[512,512]{1,0:T(8,128)(2,1)S(1)}, bf16[512,512]{1,0:T(8,128)(2,1)S(1)}, u32[]{:S(2)}, u32[]{:S(2)}) collective-permute-start(bf16[512,512]{1,0:T(8,128)(2,1)S(1)} %collective-permute-done.5.refs_3_), channel_id=1, source_target_pairs={{0,1},{1,0},{2,3},{3,2},{4,5},{5,4},{6,7},{7,6},{8,9},{9,8},{10,11... | collective-permute-start | bytes 1572872 | tf_op jit(solution)/shard_map/ppermute | solution.py:48
  127.3 111.2 %collective-permute-start.29 = (bf16[2,6,64,1024]{3,2,1,0:T(8,128)(2,1)}, bf16[2,6,64,1024]{3,2,1,0:T(8,128)(2,1)S(1)}, u32[]{:S(2)}, u32[]{:S(2)}) collective-permute-start(bf16[2,6,64,1024]{3,2,1,0:T(8,128)(2,1)} %get-tuple-element.87), channel_id=1, source_target_pairs={{0,8},{8,0},{16,24},{24,16},{1,9},{9,1},{17,25},{25,17},{2,10},{10... | collective-permute-start | bytes 4718600 | tf_op jit(solution)/shard_map/ppermute | solution.py:29
  128.9 42.3 %collective-permute-start.8 = (bf16[512,512]{1,0:T(8,128)(2,1)S(1)}, bf16[512,512]{1,0:T(8,128)(2,1)S(1)}, u32[]{:S(2)}, u32[]{:S(2)}) collective-permute-start(bf16[512,512]{1,0:T(8,128)(2,1)S(1)} %collective-permute-done.4.refs_2_), channel_id=1, source_target_pairs={{0,1},{1,0},{2,3},{3,2},{4,5},{5,4},{6,7},{7,6},{8,9},{9,8},{10,11... | collective-permute-start | bytes 1572872 | tf_op jit(solution)/shard_map/ppermute | solution.py:48
  170.7 45.8 %collective-permute-start.49 = (bf16[6,128,512]{2,1,0:T(8,128)(2,1)}, bf16[6,128,512]{2,1,0:T(8,128)(2,1)}, u32[]{:S(2)}, u32[]{:S(2)}) collective-permute-start(bf16[6,128,512]{2,1,0:T(8,128)(2,1)} %get-tuple-element.102), channel_id=1, source_target_pairs={{0,8},{8,0},{16,24},{24,16},{1,9},{9,1},{17,25},{25,17},{2,10},{10... | collective-permute-start | bytes 2359304 | tf_op jit(solution)/shard_map/ppermute | solution.py:29
  171.2 49.4 %collective-permute-start.50 = (bf16[6,128,512]{2,1,0:T(8,128)(2,1)}, bf16[6,128,512]{2,1,0:T(8,128)(2,1)}, u32[]{:S(2)}, u32[]{:S(2)}) collective-permute-start(bf16[6,128,512]{2,1,0:T(8,128)(2,1)} %get-tuple-element.103), channel_id=1, source_target_pairs={{0,16},{8,24},{16,0},{24,8},{1,17},{9,25},{17,1},{25,9},{2,18},{10... | collective-permute-start | bytes 2359304 | tf_op jit(solution)/shard_map/ppermute | solution.py:29
  173.9 102.3 %collective-permute-start.30 = (bf16[2,6,64,1024]{3,2,1,0:T(8,128)(2,1)}, bf16[2,6,64,1024]{3,2,1,0:T(8,128)(2,1)S(1)}, u32[]{:S(2)}, u32[]{:S(2)}) collective-permute-start(bf16[2,6,64,1024]{3,2,1,0:T(8,128)(2,1)} %get-tuple-element.88), channel_id=1, source_target_pairs={{0,16},{8,24},{16,0},{24,8},{1,17},{9,25},{17,1},{25,9},{2,18},{10... | collective-permute-start | bytes 4718600 | tf_op jit(solution)/shard_map/ppermute | solution.py:29
  220.6 58.0 %collective-permute-start.31 = (bf16[2,6,64,1024]{3,2,1,0:T(8,128)(2,1)}, bf16[2,6,64,1024]{3,2,1,0:T(8,128)(2,1)S(1)}, u32[]{:S(2)}, u32[]{:S(2)}) collective-permute-start(bf16[2,6,64,1024]{3,2,1,0:T(8,128)(2,1)} %get-tuple-element.89), channel_id=1, source_target_pairs={{0,24},{8,16},{16,8},{24,0},{1,25},{9,17},{17,9},{25,1},{2,26},{10... | collective-permute-start | bytes 4718600 | tf_op jit(solution)/shard_map/ppermute | solution.py:29
  220.7 70.6 %collective-permute-start.26 = (bf16[2,6,64,1024]{3,2,1,0:T(8,128)(2,1)}, bf16[2,6,64,1024]{3,2,1,0:T(8,128)(2,1)S(1)}, u32[]{:S(2)}, u32[]{:S(2)}) collective-permute-start(bf16[2,6,64,1024]{3,2,1,0:T(8,128)(2,1)} %get-tuple-element.83), channel_id=1, source_target_pairs={{0,8},{8,0},{16,24},{24,16},{1,9},{9,1},{17,25},{25,17},{2,10},{10... | collective-permute-start | bytes 4718600 | tf_op jit(solution)/shard_map/ppermute | solution.py:29
  237.1 122.9 %collective-permute-start.27 = (bf16[2,6,64,1024]{3,2,1,0:T(8,128)(2,1)}, bf16[2,6,64,1024]{3,2,1,0:T(8,128)(2,1)S(1)}, u32[]{:S(2)}, u32[]{:S(2)}) collective-permute-start(bf16[2,6,64,1024]{3,2,1,0:T(8,128)(2,1)} %get-tuple-element.84), channel_id=1, source_target_pairs={{0,16},{8,24},{16,0},{24,8},{1,17},{9,25},{17,1},{25,9},{2,18},{10... | collective-permute-start | bytes 4718600 | tf_op jit(solution)/shard_map/ppermute | solution.py:29
  238.6 121.3 %collective-permute-start.28 = (bf16[2,6,64,1024]{3,2,1,0:T(8,128)(2,1)}, bf16[2,6,64,1024]{3,2,1,0:T(8,128)(2,1)S(1)}, u32[]{:S(2)}, u32[]{:S(2)}) collective-permute-start(bf16[2,6,64,1024]{3,2,1,0:T(8,128)(2,1)} %get-tuple-element.85), channel_id=1, source_target_pairs={{0,24},{8,16},{16,8},{24,0},{1,25},{9,17},{17,9},{25,1},{2,26},{10... | collective-permute-start | bytes 4718600 | tf_op jit(solution)/shard_map/ppermute | solution.py:29
  276.2 105.9 %collective-permute-start.51 = (bf16[6,128,512]{2,1,0:T(8,128)(2,1)}, bf16[6,128,512]{2,1,0:T(8,128)(2,1)}, u32[]{:S(2)}, u32[]{:S(2)}) collective-permute-start(bf16[6,128,512]{2,1,0:T(8,128)(2,1)} %get-tuple-element.104), channel_id=1, source_target_pairs={{0,24},{8,16},{16,8},{24,0},{1,25},{9,17},{17,9},{25,1},{2,26},{10... | collective-permute-start | bytes 2359304 | tf_op jit(solution)/shard_map/ppermute | solution.py:29
  278.6 103.6 %collective-permute-start.22 = (bf16[512,320]{1,0:T(8,128)(2,1)}, bf16[512,320]{1,0:T(8,128)(2,1)S(1)}, u32[]{:S(2)}, u32[]{:S(2)}) collective-permute-start(bf16[512,320]{1,0:T(8,128)(2,1)} %get-tuple-element.81.refs_0_.refs_2_), channel_id=1, source_target_pairs={{0,1},{1,0},{2,3},{3,2},{4,5},{5,4},{6,7},{7,6},{8,9},{9,8},{10,11... | collective-permute-start | bytes 983048 | tf_op jit(solution)/shard_map/ppermute | solution.py:48
  291.3 93.4 %collective-permute-start.19 = (bf16[512,320]{1,0:T(8,128)(2,1)}, bf16[512,320]{1,0:T(8,128)(2,1)S(1)}, u32[]{:S(2)}, u32[]{:S(2)}) collective-permute-start(bf16[512,320]{1,0:T(8,128)(2,1)} %get-tuple-element.81.refs_0_.refs_2_), channel_id=1, source_target_pairs={{0,2},{1,3},{2,0},{3,1},{4,6},{5,7},{6,4},{7,5},{8,10},{9,11},{10,... | collective-permute-start | bytes 983048 | tf_op jit(solution)/shard_map/ppermute | solution.py:42
  384.7 53.1 %collective-permute-start.33 = (bf16[512,384]{1,0:T(8,128)(2,1)}, bf16[512,384]{1,0:T(8,128)(2,1)S(1)}, u32[]{:S(2)}, u32[]{:S(2)}) collective-permute-start(bf16[512,384]{1,0:T(8,128)(2,1)} %get-tuple-element.94.refs_2_), channel_id=1, source_target_pairs={{0,4},{1,5},{2,6},{3,7},{4,0},{5,1},{6,2},{7,3},{8,12},{9,13},{10,... | collective-permute-start | bytes 1179656 | tf_op jit(solution)/shard_map/ppermute | solution.py:42
  388.2 49.7 %collective-permute-start.32 = (bf16[512,384]{1,0:T(8,128)(2,1)}, bf16[512,384]{1,0:T(8,128)(2,1)S(1)}, u32[]{:S(2)}, u32[]{:S(2)}) collective-permute-start(bf16[512,384]{1,0:T(8,128)(2,1)} %get-tuple-element.94.refs_2_), channel_id=1, source_target_pairs={{0,2},{1,3},{2,0},{3,1},{4,6},{5,7},{6,4},{7,5},{8,10},{9,11},{10,... | collective-permute-start | bytes 1179656 | tf_op jit(solution)/shard_map/ppermute | solution.py:42
  389.9 48.1 %collective-permute-start.42 = (bf16[512,384]{1,0:T(8,128)(2,1)S(1)}, bf16[512,384]{1,0:T(8,128)(2,1)S(1)}, u32[]{:S(2)}, u32[]{:S(2)}) collective-permute-start(bf16[512,384]{1,0:T(8,128)(2,1)S(1)} %copy-done.26), channel_id=1, source_target_pairs={{0,1},{1,0},{2,3},{3,2},{4,5},{5,4},{6,7},{7,6},{8,9},{9,8},{10,11... | collective-permute-start | bytes 1179656 | tf_op jit(solution)/shard_map/ppermute | solution.py:48
  390.0 48.4 %collective-permute-start.41 = (bf16[512,384]{1,0:T(8,128)(2,1)S(1)}, bf16[512,384]{1,0:T(8,128)(2,1)S(1)}, u32[]{:S(2)}, u32[]{:S(2)}) collective-permute-start(bf16[512,384]{1,0:T(8,128)(2,1)S(1)} %copy-done.26), channel_id=1, source_target_pairs={{0,6},{1,7},{2,4},{3,5},{4,2},{5,3},{6,0},{7,1},{8,14},{9,15},{10,... | collective-permute-start | bytes 1179656 | tf_op jit(solution)/shard_map/ppermute | solution.py:42
  396.4 58.4 %collective-permute-start.40 = (bf16[512,384]{1,0:T(8,128)(2,1)S(1)}, bf16[512,384]{1,0:T(8,128)(2,1)S(1)}, u32[]{:S(2)}, u32[]{:S(2)}) collective-permute-start(bf16[512,384]{1,0:T(8,128)(2,1)S(1)} %copy-done.26), channel_id=1, source_target_pairs={{0,4},{1,5},{2,6},{3,7},{4,0},{5,1},{6,2},{7,3},{8,12},{9,13},{10,... | collective-permute-start | bytes 1179656 | tf_op jit(solution)/shard_map/ppermute | solution.py:42
  460.3 35.2 %collective-permute-start.55 = (bf16[2,128,512]{2,1,0:T(8,128)(2,1)}, bf16[2,128,512]{2,1,0:T(8,128)(2,1)}, u32[]{:S(2)}, u32[]{:S(2)}) collective-permute-start(bf16[2,128,512]{2,1,0:T(8,128)(2,1)} %get-tuple-element.114), channel_id=1, source_target_pairs={{0,8},{8,0},{16,24},{24,16},{1,9},{9,1},{17,25},{25,17},{2,10},{10... | collective-permute-start | bytes 786440 | tf_op jit(solution)/shard_map/ppermute | solution.py:29
  460.9 36.2 %collective-permute-start.56 = (bf16[2,128,512]{2,1,0:T(8,128)(2,1)}, bf16[2,128,512]{2,1,0:T(8,128)(2,1)}, u32[]{:S(2)}, u32[]{:S(2)}) collective-permute-start(bf16[2,128,512]{2,1,0:T(8,128)(2,1)} %get-tuple-element.115), channel_id=1, source_target_pairs={{0,16},{8,24},{16,0},{24,8},{1,17},{9,25},{17,1},{25,9},{2,18},{10... | collective-permute-start | bytes 786440 | tf_op jit(solution)/shard_map/ppermute | solution.py:29
  461.7 35.4 %collective-permute-start.57 = (bf16[2,128,512]{2,1,0:T(8,128)(2,1)}, bf16[2,128,512]{2,1,0:T(8,128)(2,1)}, u32[]{:S(2)}, u32[]{:S(2)}) collective-permute-start(bf16[2,128,512]{2,1,0:T(8,128)(2,1)} %get-tuple-element.116), channel_id=1, source_target_pairs={{0,24},{8,16},{16,8},{24,0},{1,25},{9,17},{17,9},{25,1},{2,26},{10... | collective-permute-start | bytes 786440 | tf_op jit(solution)/shard_map/ppermute | solution.py:29
  466.5 37.8 %collective-permute-start.63 = (bf16[128,512]{1,0:T(8,128)(2,1)}, bf16[128,512]{1,0:T(8,128)(2,1)S(1)}, u32[]{:S(2)}, u32[]{:S(2)}) collective-permute-start(bf16[128,512]{1,0:T(8,128)(2,1)} %convert_element_type.23.refs_8_.refs_0_), channel_id=1, source_target_pairs={{0,24},{8,16},{16,8},{24,0},{1,25},{9,17},{17,9},{25,1},{2,26},{10... | collective-permute-start | bytes 393224 | tf_op jit(solution)/shard_map/ppermute | solution.py:29
  (91 other events, 2796.2 us)
where the time goes:
time: 513 us; the launch traced here: 512 us
  waiting for transfers between devices  290 us (57%)
  Pallas kernels  118 us (23%)
  starting transfers between devices  88.5 us (17%)
  other arithmetic  7.54 us (1%)
  local copies, waits for them, and re-layouts  6.05 us (1%)
    ppermute x33, waiting for transfers between devices, exchange(): return lax.ppermute(x, axis, [(i, partner(i, s, n)[0]) for i in range(n)])  193 us
    ppermute x12, waiting for transfers between devices, gather_z(): got.append(lax.ppermute(x, 'tp', pairs))  94.5 us
    ppermute x33, starting transfers between devices, exchange(): return lax.ppermute(x, axis, [(i, partner(i, s, n)[0]) for i in range(n)])  42.7 us
    ppermute x12, starting transfers between devices, gather_z(): got.append(lax.ppermute(x, 'tp', pairs))  40.1 us
    pallas_call x3, Pallas kernels, gu_step(): pl.pallas_call(functools.partial(gu_body, n, lo, count, shared, not prev)...  30.8 us
    pallas_call x4, Pallas kernels, down_step(): pl.pallas_call(functools.partial(down_body, n, parts, lo, count, skip, fi...  29.3 us
    pallas_call x3, Pallas kernels, prep_gu(): pl.pallas_call(functools.partial(prep_gu_body, n), grid_spec=pltpu.Prefet...  24.2 us
    pallas_call x4, Pallas kernels, prep_down(): pl.pallas_call(functools.partial(prep_down_body, n), grid_spec=pltpu.Pref...  19.3 us
  transfers between devices with their start and end apart: 64, of which 21 were waited for; matrix products, arithmetic and copies ran while one was open for 1% of the time, Pallas kernels for 23%

commit v1 on v0

--- a/solution.py
+++ b/solution.py
@@ -82,7 +82,7 @@
 def prep_gu(gate, up, gain, base, lo, count, token):
     n = base.shape[0]
     _, hp, df = gate.shape
-    block = lambda s: pl.BlockSpec((1, hp, df), lambda i, idx, s=s: (idx[s] + i, 0, 0))
+    block = lambda s: pl.BlockSpec((1, hp, df), lambda i, idx, s=s: (idx[s] + lo + i, 0, 0))
     return pl.pallas_call(
         functools.partial(prep_gu_body, n),
         grid_spec=pltpu.PrefetchScalarGridSpec(
@@ -96,7 +96,7 @@
         ),
         out_shape=[jax.ShapeDtypeStruct((2, count, hp, df), jnp.bfloat16)] * n + [TOKEN],
         compiler_params=pltpu.CompilerParams(vmem_limit_bytes=VMEM_LIMIT),
-    )(base + lo, gain, *([gate] * n), *([up] * n), token)
+    )(base, gain, *([gate] * n), *([up] * n), token)
 
 
 def prep_down_body(n, idx_ref, *refs):
@@ -108,7 +108,7 @@
 def prep_down(down, base, lo, count, token):
     n = base.shape[0]
     _, hf, dp = down.shape
-    block = lambda s: pl.BlockSpec((1, hf, dp), lambda i, idx, s=s: (idx[s] + i, 0, 0))
+    block = lambda s: pl.BlockSpec((1, hf, dp), lambda i, idx, s=s: (idx[s] + lo + i, 0, 0))
     return pl.pallas_call(
         functools.partial(prep_down_body, n),
         grid_spec=pltpu.PrefetchScalarGridSpec(
@@ -120,7 +120,7 @@
         ),
         out_shape=[jax.ShapeDtypeStruct((count, hf, dp), jnp.bfloat16)] * n + [TOKEN],
         compiler_params=pltpu.CompilerParams(vmem_limit_bytes=VMEM_LIMIT),
-    )(base + lo, *([down] * n), token)
+    )(base, *([down] * n), token)
 
 
 def pack_body(n, *refs):
@@ -343,6 +343,54 @@
         take(1)
     (down_out,) = take(1)
     results = take(n) if last else take(1)
+    buf, a_buf, acc, in_sem, a_sem, out_sem = refs
+    share = parts // n
+    _, _, hp, dp = buf.shape
+    lanes = count * hp
+    copies = []
+    for s in range(n):
+        for j in range(share):
+            part = blk_ref[s] * share + j
+            rows = pieces[s].at[:, pl.ds(j * hp, hp), :]
+            copies.append(pltpu.make_async_copy(rows, buf.at[part], in_sem.at[s, j]))
+    for k in range(parts):
+        source = gathered[k].at[:, pl.ds(skip * hp, lanes)]
+        copies.append(pltpu.make_async_copy(source, a_buf.at[from_ref[k]], a_sem.at[k]))
+    copies.append(pltpu.make_async_copy(acc_in, acc, a_sem.at[parts]))
+    for copy in copies:
+        copy.start()
+    for copy in copies:
+        copy.wait()
+    out = []
+    for p in range(parts):
+        rows = down_out.at[pl.ds(lo, count), pl.ds(p * hp, hp), :]
+        out.append(pltpu.make_async_copy(buf.at[p], rows, out_sem.at[p]))
+    for copy in out:
+        copy.start()
+    left = jnp.concatenate([a_buf[p] for p in range(parts)], axis=1)
+    right = buf[...].reshape(parts * lanes, dp)
+    total = acc[...] + jnp.dot(left, right, preferred_element_type=jnp.float32)
+    own = acc.shape[0] // n
+    if last:
+        for r in range(n):
+            results[r][...] = total[r * own : (r + 1) * own].astype(results[r].dtype)
+    else:
+        results[0][...] = total
+    for copy in out:
+        copy.wait()
+
+
+def down_body_narrow(n, parts, lo, count, skip, first, last, *refs):
+    refs = list(refs)
+    take = lambda k: [refs.pop(0) for _ in range(k)]
+    from_ref, blk_ref = take(2)
+    gathered = take(parts)
+    (acc_in,) = take(1)
+    pieces = take(n)
+    if not first:
+        take(1)
+    (down_out,) = take(1)
+    results = take(n) if last else take(1)
     buf, in_sem, out_sem = refs
     hf = pieces[0].shape[1]
     copies = []
@@ -379,6 +427,8 @@
     rows = acc.shape[0]
     own = rows // n
     hidden = hf * n
+    hp = hidden // parts
+    share = parts // n
     first = prev is None
     bf = jnp.bfloat16
     out_shape = [jax.ShapeDtypeStruct((n_local, hidden, dp), bf)]
@@ -388,16 +438,31 @@
     else:
         out_shape.append(jax.ShapeDtypeStruct((rows, dp), jnp.float32))
     args = [source, blk, *gathered, acc, *pieces] + ([] if first else [prev])
-    return pl.pallas_call(
-        functools.partial(down_body, n, parts, lo, count, skip, first, last),
-        in_specs=[SMEM] * 2 + [VMEM] * (parts + 1) + [ANY] * (len(args) - parts - 3),
-        out_specs=[ANY] + [VMEM] * (len(out_shape) - 1),
-        out_shape=out_shape,
-        scratch_shapes=[
+    specs = [SMEM] * 2 + [ANY] * (len(args) - 2)
+    if count * hp % 128 == 0 and skip * hp % 128 == 0 and share * hp == hf:
+        kernel = down_body
+        scratch = [
+            pltpu.VMEM((parts, count, hp, dp), bf),
+            pltpu.VMEM((parts, rows, count * hp), bf),
+            pltpu.VMEM((rows, dp), jnp.float32),
+            pltpu.SemaphoreType.DMA((n, share)),
+            pltpu.SemaphoreType.DMA((parts + 1,)),
+            pltpu.SemaphoreType.DMA((parts,)),
+        ]
+    else:
+        kernel = down_body_narrow
+        specs[2 : parts + 3] = [VMEM] * (parts + 1)
+        scratch = [
             pltpu.VMEM((count, hidden, dp), bf),
             pltpu.SemaphoreType.DMA((n,)),
             pltpu.SemaphoreType.DMA,
-        ],
+        ]
+    return pl.pallas_call(
+        functools.partial(kernel, n, parts, lo, count, skip, first, last),
+        in_specs=specs,
+        out_specs=[ANY] + [VMEM] * (len(out_shape) - 1),
+        out_shape=out_shape,
+        scratch_shapes=scratch,
         input_output_aliases={} if first else {len(args) - 1: 0},
         compiler_params=pltpu.CompilerParams(vmem_limit_bytes=VMEM_LIMIT),
     )(*args)
@@ -437,7 +502,7 @@
     tables = swap([table] * n)
     chunks = cuts(n_local)
     steps = down_cuts(chunks)
-    token = jnp.zeros(TOKEN.shape, TOKEN.dtype)
+    token = tokens
     gu, down = {}, {}
     for c, (lo, count) in enumerate(chunks):
         *pieces, token = prep_gu(gate_train, up_train, gain, base, lo, count, token)
@@ -448,6 +513,8 @@
     for i, (_, lo, count) in enumerate(steps):
         *pieces, token = prep_down(down_train, base, lo, count, token)
         down[i] = swap(pieces)
+        if i == 0:
+            first_token = token
     own_shared_down = shared_down_train.astype(bf)
     shared_down = swap([own_shared_down] * n)
 
@@ -459,7 +526,7 @@
     for c, (lo, count) in enumerate(chunks):
         results = gu_step(
             *(blk, x, inv, w, gu[c], shared_gu if c == 0 else []),
-            *(prev, token, lo, count, n_local, width),
+            *(prev, first_token, lo, count, n_local, width),
         )
         if c == 0:
             shared_gate_serve, shared_up_serve = results[2:4]

time: 513 us -> 502 us (0.979)
  starting transfers between devices: 88.5 us -> 82.2 us
  Pallas kernels: 118 us -> 112 us
    ppermute x12, starting transfers between devices: 40.1 us -> 29.6 us  [gather_z(): got.append(lax.ppermute(x, 'tp', pairs))]
    pallas_call x4, Pallas kernels: 29.3 us -> 23.2 us  [down_step(): pl.pallas_call(functools.partial(kernel, n, parts, lo, count, skip, first...]
  transfers between devices with their start and end apart: 64 -> 64, of which waited for: 21 -> 22; matrix products, arithmetic and copies ran while one was open for 1% -> 1% of each run, Pallas kernels for 23% -> 23%
where the time goes in v1:
time: 502 us; the launch traced here: 497 us
  waiting for transfers between devices  288 us (57%)
  Pallas kernels  112 us (22%)
  starting transfers between devices  82.2 us (16%)
  other arithmetic  6.96 us (1%)
  local copies, waits for them, and re-layouts  6.38 us (1%)
    ppermute x33, waiting for transfers between devices, exchange(): return lax.ppermute(x, axis, [(i, partner(i, s, n)[0]) for i in range(n)])  190 us
    ppermute x12, waiting for transfers between devices, gather_z(): got.append(lax.ppermute(x, 'tp', pairs))  93.3 us
    ppermute x33, starting transfers between devices, exchange(): return lax.ppermute(x, axis, [(i, partner(i, s, n)[0]) for i in range(n)])  46.3 us
    pallas_call x3, Pallas kernels, gu_step(): pl.pallas_call(functools.partial(gu_body, n, lo, count, shared, not prev)...  30.7 us
    ppermute x12, starting transfers between devices, gather_z(): got.append(lax.ppermute(x, 'tp', pairs))  29.6 us
    pallas_call x3, Pallas kernels, prep_gu(): pl.pallas_call(functools.partial(prep_gu_body, n), grid_spec=pltpu.Prefet...  24.3 us
    pallas_call x4, Pallas kernels, down_step(): pl.pallas_call(functools.partial(kernel, n, parts, lo, count, skip, first...  23.2 us
    pallas_call x4, Pallas kernels, prep_down(): pl.pallas_call(functools.partial(prep_down_body, n), grid_spec=pltpu.Pref...  19.3 us
  transfers between devices with their start and end apart: 64, of which 22 were waited for; matrix products, arithmetic and copies ran while one was open for 1% of the time, Pallas kernels for 23%

profile of v1, /device:TPU:0, one launch (start us, length us, event | category | flops | bytes accessed | tf_op | source)
XLA Modules:
  0.0 496.9 jit_solution(13099642310093317962)
XLA Ops:
  12.3 6.4 %shard_map.153 = (bf16[2,4,64,1024]{3,2,1,0:T(8,128)(2,1)}, bf16[2,4,64,1024]{3,2,1,0:T(8,128)(2,1)}, bf16[2,4,64,1024]{3,2,1,0:T(8,128)(2,1)}, bf16[2,4,64,1024]{3,2,1,0:T(8,128)(2,1)}, f32[8,128]{1,0:T(8,128)}) custom-call(s32[4]{0:T(128)} %get-tuple-element.125.idx_ref, f32[1,1024]{1,0:T(1,128)} %bitcast.20, f32[64,64,1024]{2,1,0:T(8,128)} %refs_3_.9, ...), custom_call_target="tpu_custom_call" | custom-call | tf_op jit(solution)/shard_map/pallas_call | solution.py:86
  21.5 8.9 %shard_map.154 = (bf16[2,6,64,1024]{3,2,1,0:T(8,128)(2,1)}, bf16[2,6,64,1024]{3,2,1,0:T(8,128)(2,1)}, bf16[2,6,64,1024]{3,2,1,0:T(8,128)(2,1)}, bf16[2,6,64,1024]{3,2,1,0:T(8,128)(2,1)}, f32[8,128]{1,0:T(8,128)}) custom-call(s32[4]{0:T(128)} %get-tuple-element.125.idx_ref, f32[1,1024]{1,0:T(1,128)} %bitcast.21, f32[64,64,1024]{2,1,0:T(8,128)} %refs_3_.9, ...), custom_call_target="tpu_custom_call" | custom-call | tf_op jit(solution)/shard_map/pallas_call | solution.py:86
  30.4 8.9 %shard_map.155 = (bf16[2,6,64,1024]{3,2,1,0:T(8,128)(2,1)}, bf16[2,6,64,1024]{3,2,1,0:T(8,128)(2,1)}, bf16[2,6,64,1024]{3,2,1,0:T(8,128)(2,1)}, bf16[2,6,64,1024]{3,2,1,0:T(8,128)(2,1)}, f32[8,128]{1,0:T(8,128)}) custom-call(s32[4]{0:T(128)} %get-tuple-element.125.idx_ref, f32[1,1024]{1,0:T(1,128)} %bitcast.22, f32[64,64,1024]{2,1,0:T(8,128)} %refs_3_.9, ...), custom_call_target="tpu_custom_call" | custom-call | tf_op jit(solution)/shard_map/pallas_call | solution.py:86
  39.4 6.6 %shard_map.156 = (bf16[6,128,512]{2,1,0:T(8,128)(2,1)}, bf16[6,128,512]{2,1,0:T(8,128)(2,1)}, bf16[6,128,512]{2,1,0:T(8,128)(2,1)}, bf16[6,128,512]{2,1,0:T(8,128)(2,1)}, f32[8,128]{1,0:T(8,128)}) custom-call(s32[4]{0:T(128)} %get-tuple-element.125.idx_ref, f32[64,128,512]{2,1,0:T(8,128)} %refs_3_.13, f32[64,128,512]{2,1,0:T(8,128)} %refs_3_.13, ...), custom_call_target="tpu_custom_call" | custom-call | tf_op jit(solution)/shard_map/pallas_call | solution.py:112
  45.9 6.5 %shard_map.161 = (bf16[6,128,512]{2,1,0:T(8,128)(2,1)}, bf16[6,128,512]{2,1,0:T(8,128)(2,1)}, bf16[6,128,512]{2,1,0:T(8,128)(2,1)}, bf16[6,128,512]{2,1,0:T(8,128)(2,1)}, f32[8,128]{1,0:T(8,128)}) custom-call(s32[4]{0:T(128)} %get-tuple-element.125.idx_ref, f32[64,128,512]{2,1,0:T(8,128)} %refs_3_.13, f32[64,128,512]{2,1,0:T(8,128)} %refs_3_.13, ...), custom_call_target="tpu_custom_call" | custom-call | tf_op jit(solution)/shard_map/pallas_call | solution.py:112
  52.5 3.2 shard_map.163
  57.8 4.9 collective-permute-done.10.refs_9_
  77.2 7.2 %collective-permute-done.53.refs_13_ = bf16[2,128,512]{2,1,0:T(8,128)(2,1)S(1)} collective-permute-done((bf16[2,128,512]{2,1,0:T(8,128)(2,1)}, bf16[2,128,512]{2,1,0:T(8,128)(2,1)S(1)}, u32[]{:S(2)}, u32[]{:S(2)}) %collective-permute-start.53) | collective-permute-done | bytes 262176 | tf_op jit(solution)/shard_map/ppermute | solution.py:29
  90.8 19.8 %collective-permute-done.4.refs_2_ = bf16[512,512]{1,0:T(8,128)(2,1)S(1)} collective-permute-done((bf16[512,512]{1,0:T(8,128)(2,1)S(1)}, bf16[512,512]{1,0:T(8,128)(2,1)S(1)}, u32[]{:S(2)}, u32[]{:S(2)}) %collective-permute-start.4) | collective-permute-done | bytes 524320 | tf_op jit(solution)/shard_map/ppermute | solution.py:42
  116.0 11.4 %collective-permute-done.46.refs_12_ = bf16[6,128,512]{2,1,0:T(8,128)(2,1)S(1)} collective-permute-done((bf16[6,128,512]{2,1,0:T(8,128)(2,1)S(1)}, bf16[6,128,512]{2,1,0:T(8,128)(2,1)S(1)}, u32[]{:S(2)}, u32[]{:S(2)}) %collective-permute-start.46) | collective-permute-done | bytes 786464 | tf_op jit(solution)/shard_map/ppermute | solution.py:29
  129.3 27.0 %collective-permute-done.14.refs_6_ = bf16[2,4,64,1024]{3,2,1,0:T(8,128)(2,1)S(1)} collective-permute-done((bf16[2,4,64,1024]{3,2,1,0:T(8,128)(2,1)}, bf16[2,4,64,1024]{3,2,1,0:T(8,128)(2,1)S(1)}, u32[]{:S(2)}, u32[]{:S(2)}) %collective-permute-start.14) | collective-permute-done | bytes 1048608 | tf_op jit(solution)/shard_map/ppermute | solution.py:29
  163.2 7.4 %route.1 = (bf16[8,512,512]{2,1,0:T(8,128)(2,1)}, f32[512,1024]{1,0:T(8,128)}, f32[512,1]{1,0:T(8,128)}) custom-call(s32[1]{0:T(128)} %bitcast.8.me_ref, s32[8]{0:T(128)} %stack.64.from_ref.refs_0_, bf16[512,512]{1,0:T(8,128)(2,1)} %pack_tokens.1.refs_0_.refs_8_, bf16[512,512]{1,0:T(8,128)(2,1)} %copy-done.19, bf16[512,512]{1,0:T(8,128)(2,1)} %copy-done.20, ...), custom_call_target="tpu_custom_call" | custom-call | tf_op jit(solution)/shard_map/route/pallas_call | solution.py:170
  170.6 10.3 %shard_map.157 = (bf16[16,64,4096]{2,1,0:T(8,128)(2,1)}, bf16[16,64,4096]{2,1,0:T(8,128)(2,1)}, bf16[64,4096]{1,0:T(8,128)(2,1)}, bf16[64,4096]{1,0:T(8,128)(2,1)}, bf16[512,320]{1,0:T(8,128)(2,1)}) custom-call(s32[4]{0:T(128)} %get-tuple-element.126.refs_0_.refs_1_.blk_ref, bf16[8,512,512]{2,1,0:T(8,128)(2,1)} %get-tuple-element.67.refs_1_, ...), custom_call_target="tpu_custom_call" | custom-call | tf_op jit(solution)/shard_map/pallas_call | solution.py:318
  181.0 20.8 %collective-permute-done.48.refs_14_ = bf16[6,128,512]{2,1,0:T(8,128)(2,1)} collective-permute-done((bf16[6,128,512]{2,1,0:T(8,128)(2,1)}, bf16[6,128,512]{2,1,0:T(8,128)(2,1)}, u32[]{:S(2)}, u32[]{:S(2)}) %collective-permute-start.48) | collective-permute-done | bytes 786464 | tf_op jit(solution)/shard_map/ppermute | solution.py:29
  201.8 5.5 %collective-permute-start.19 = (bf16[512,320]{1,0:T(8,128)(2,1)}, bf16[512,320]{1,0:T(8,128)(2,1)S(1)}, u32[]{:S(2)}, u32[]{:S(2)}) collective-permute-start(bf16[512,320]{1,0:T(8,128)(2,1)} %get-tuple-element.77.refs_0_.refs_2_), channel_id=1, source_target_pairs={{0,2},{1,3},{2,0},{3,1},{4,6},{5,7},{6,4},{7,5},{8,10},{9,11},{10,... | collective-permute-start | bytes 983048 | tf_op jit(solution)/shard_map/ppermute | solution.py:42
  207.3 8.8 %collective-permute-done.49.refs_12_ = bf16[6,128,512]{2,1,0:T(8,128)(2,1)} collective-permute-done((bf16[6,128,512]{2,1,0:T(8,128)(2,1)}, bf16[6,128,512]{2,1,0:T(8,128)(2,1)}, u32[]{:S(2)}, u32[]{:S(2)}) %collective-permute-start.49) | collective-permute-done | bytes 786464 | tf_op jit(solution)/shard_map/ppermute | solution.py:29
  221.0 14.4 %collective-permute-done.20.refs_2_.refs_4_ = bf16[512,320]{1,0:T(8,128)(2,1)S(1)} collective-permute-done((bf16[512,320]{1,0:T(8,128)(2,1)}, bf16[512,320]{1,0:T(8,128)(2,1)S(1)}, u32[]{:S(2)}, u32[]{:S(2)}) %collective-permute-start.20) | collective-permute-done | bytes 327712 | tf_op jit(solution)/shard_map/ppermute | solution.py:42
  238.5 25.8 %collective-permute-done.27.refs_6_ = bf16[2,6,64,1024]{3,2,1,0:T(8,128)(2,1)S(1)} collective-permute-done((bf16[2,6,64,1024]{3,2,1,0:T(8,128)(2,1)}, bf16[2,6,64,1024]{3,2,1,0:T(8,128)(2,1)S(1)}, u32[]{:S(2)}, u32[]{:S(2)}) %collective-permute-start.27) | collective-permute-done | bytes 1572896 | tf_op jit(solution)/shard_map/ppermute | solution.py:29
  267.8 22.3 %collective-permute-done.29.refs_5_ = bf16[2,6,64,1024]{3,2,1,0:T(8,128)(2,1)S(1)} collective-permute-done((bf16[2,6,64,1024]{3,2,1,0:T(8,128)(2,1)}, bf16[2,6,64,1024]{3,2,1,0:T(8,128)(2,1)S(1)}, u32[]{:S(2)}, u32[]{:S(2)}) %collective-permute-start.29) | collective-permute-done | bytes 1572896 | tf_op jit(solution)/shard_map/ppermute | solution.py:29
  290.1 58.0 %collective-permute-done.30.refs_6_ = bf16[2,6,64,1024]{3,2,1,0:T(8,128)(2,1)S(1)} collective-permute-done((bf16[2,6,64,1024]{3,2,1,0:T(8,128)(2,1)}, bf16[2,6,64,1024]{3,2,1,0:T(8,128)(2,1)S(1)}, u32[]{:S(2)}, u32[]{:S(2)}) %collective-permute-start.30) | collective-permute-done | bytes 1572896 | tf_op jit(solution)/shard_map/ppermute | solution.py:29
  349.8 10.3 %shard_map.158 = (bf16[16,64,4096]{2,1,0:T(8,128)(2,1)}, bf16[16,64,4096]{2,1,0:T(8,128)(2,1)}, bf16[512,384]{1,0:T(8,128)(2,1)}) custom-call(s32[4]{0:T(128)} %get-tuple-element.126.refs_0_.refs_1_.blk_ref, bf16[8,512,512]{2,1,0:T(8,128)(2,1)} %get-tuple-element.67.refs_1_, ...), custom_call_target="tpu_custom_call", output_to_operand_aliasing={{0}: (8, {}), {1}: (9, {})} | custom-call | tf_op jit(solution)/shard_map/pallas_call | solution.py:318
  360.1 10.1 %shard_map.159 = (bf16[16,64,4096]{2,1,0:T(8,128)(2,1)}, bf16[16,64,4096]{2,1,0:T(8,128)(2,1)}, bf16[512,384]{1,0:T(8,128)(2,1)}) custom-call(s32[4]{0:T(128)} %get-tuple-element.126.refs_0_.refs_1_.blk_ref, bf16[8,512,512]{2,1,0:T(8,128)(2,1)} %get-tuple-element.67.refs_1_, ...), custom_call_target="tpu_custom_call", output_to_operand_aliasing={{0}: (8, {}), {1}: (9, {})} | custom-call | tf_op jit(solution)/shard_map/pallas_call | solution.py:318
  370.2 10.4 %collective-permute-start.32 = (bf16[512,384]{1,0:T(8,128)(2,1)}, bf16[512,384]{1,0:T(8,128)(2,1)S(1)}, u32[]{:S(2)}, u32[]{:S(2)}) collective-permute-start(bf16[512,384]{1,0:T(8,128)(2,1)} %get-tuple-element.90.refs_2_), channel_id=1, source_target_pairs={{0,2},{1,3},{2,0},{3,1},{4,6},{5,7},{6,4},{7,5},{8,10},{9,11},{10,... | collective-permute-start | bytes 1179656 | tf_op jit(solution)/shard_map/ppermute | solution.py:42
  385.9 12.4 %collective-permute-done.32.refs_3_ = bf16[512,384]{1,0:T(8,128)(2,1)S(1)} collective-permute-done((bf16[512,384]{1,0:T(8,128)(2,1)}, bf16[512,384]{1,0:T(8,128)(2,1)S(1)}, u32[]{:S(2)}, u32[]{:S(2)}) %collective-permute-start.32) | collective-permute-done | bytes 393248 | tf_op jit(solution)/shard_map/ppermute | solution.py:42
  398.4 12.2 %collective-permute-done.33.refs_4_ = bf16[512,384]{1,0:T(8,128)(2,1)S(1)} collective-permute-done((bf16[512,384]{1,0:T(8,128)(2,1)}, bf16[512,384]{1,0:T(8,128)(2,1)S(1)}, u32[]{:S(2)}, u32[]{:S(2)}) %collective-permute-start.33) | collective-permute-done | bytes 393248 | tf_op jit(solution)/shard_map/ppermute | solution.py:42
  415.7 28.7 %collective-permute-done.40.refs_4_ = bf16[512,384]{1,0:T(8,128)(2,1)} collective-permute-done((bf16[512,384]{1,0:T(8,128)(2,1)S(1)}, bf16[512,384]{1,0:T(8,128)(2,1)}, u32[]{:S(2)}, u32[]{:S(2)}) %collective-permute-start.40) | collective-permute-done | bytes 393248 | tf_op jit(solution)/shard_map/ppermute | solution.py:42
  446.3 3.1 shard_map.165
  456.6 3.6 shared_down.1.refs_10_
  460.1 6.8 %shard_map.160 = (bf16[16,512,512]{2,1,0:T(8,128)(2,1)}, f32[512,512]{1,0:T(8,128)}) custom-call(s32[8]{0:T(128)} %stack.64.from_ref.refs_0_, s32[4]{0:T(128)} %get-tuple-element.126.refs_0_.refs_1_.blk_ref, bf16[512,384]{1,0:T(8,128)(2,1)} %get-tuple-element.91.refs_2_, bf16[512,384]{1,0:T(8,128)(2,1)} %collective-permute-done.39.refs_3_, ...), custom_call_target="tpu_custom_call" | custom-call | tf_op jit(solution)/shard_map/pallas_call | solution.py:460
  466.9 6.8 %shard_map.162 = (bf16[16,512,512]{2,1,0:T(8,128)(2,1)}, f32[512,512]{1,0:T(8,128)}) custom-call(s32[8]{0:T(128)} %stack.64.from_ref.refs_0_, s32[4]{0:T(128)} %get-tuple-element.126.refs_0_.refs_1_.blk_ref, bf16[512,384]{1,0:T(8,128)(2,1)} %get-tuple-element.90.refs_2_, bf16[512,384]{1,0:T(8,128)(2,1)} %copy-done.27, ...), custom_call_target="tpu_custom_call", output_to_operand_aliasing={{0}: (15, {})} | custom-call | tf_op jit(solution)/shard_map/pallas_call | solution.py:460
  475.4 4.8 shard_map.164
  482.7 4.7 shard_map.166
  (231 shorter events, 97.2 us)
Async XLA Ops:
  7.0 65.7 %collective-permute-start.16 = (bf16[2,64,1024]{2,1,0:T(8,128)(2,1)}, bf16[2,64,1024]{2,1,0:T(8,128)(2,1)}, u32[]{:S(2)}, u32[]{:S(2)}) collective-permute-start(bf16[2,64,1024]{2,1,0:T(8,128)(2,1)} %fusion.refs_8_), channel_id=1, source_target_pairs={{0,8},{8,0},{16,24},{24,16},{1,9},{9,1},{17,25},{25,17},{2,10},{10... | collective-permute-start | bytes 786440 | tf_op jit(solution)/shard_map/ppermute | solution.py:29
  8.9 66.4 %collective-permute-start.17 = (bf16[2,64,1024]{2,1,0:T(8,128)(2,1)}, bf16[2,64,1024]{2,1,0:T(8,128)(2,1)}, u32[]{:S(2)}, u32[]{:S(2)}) collective-permute-start(bf16[2,64,1024]{2,1,0:T(8,128)(2,1)} %fusion.refs_8_), channel_id=1, source_target_pairs={{0,16},{8,24},{16,0},{24,8},{1,17},{9,25},{17,1},{25,9},{2,18},{10... | collective-permute-start | bytes 786440 | tf_op jit(solution)/shard_map/ppermute | solution.py:29
  18.8 56.6 %collective-permute-start.18 = (bf16[2,64,1024]{2,1,0:T(8,128)(2,1)}, bf16[2,64,1024]{2,1,0:T(8,128)(2,1)S(1)}, u32[]{:S(2)}, u32[]{:S(2)}) collective-permute-start(bf16[2,64,1024]{2,1,0:T(8,128)(2,1)} %fusion.refs_8_), channel_id=1, source_target_pairs={{0,24},{8,16},{16,8},{24,0},{1,25},{9,17},{17,9},{25,1},{2,26},{10... | collective-permute-start | bytes 786440 | tf_op jit(solution)/shard_map/ppermute | solution.py:29
  72.7 37.9 %collective-permute-start.4 = (bf16[512,512]{1,0:T(8,128)(2,1)S(1)}, bf16[512,512]{1,0:T(8,128)(2,1)S(1)}, u32[]{:S(2)}, u32[]{:S(2)}) collective-permute-start(bf16[512,512]{1,0:T(8,128)(2,1)S(1)} %copy-done), channel_id=1, source_target_pairs={{0,4},{1,5},{2,6},{3,7},{4,0},{5,1},{6,2},{7,3},{8,12},{9,13},{10,... | collective-permute-start | bytes 1572872 | tf_op jit(solution)/shard_map/ppermute | solution.py:42
  75.3 36.9 %collective-permute-start.5 = (bf16[512,512]{1,0:T(8,128)(2,1)S(1)}, bf16[512,512]{1,0:T(8,128)(2,1)S(1)}, u32[]{:S(2)}, u32[]{:S(2)}) collective-permute-start(bf16[512,512]{1,0:T(8,128)(2,1)S(1)} %copy-done), channel_id=1, source_target_pairs={{0,6},{1,7},{2,4},{3,5},{4,2},{5,3},{6,0},{7,1},{8,14},{9,15},{10,... | collective-permute-start | bytes 1572872 | tf_op jit(solution)/shard_map/ppermute | solution.py:42
  75.4 37.4 %collective-permute-start.6 = (bf16[512,512]{1,0:T(8,128)(2,1)S(1)}, bf16[512,512]{1,0:T(8,128)(2,1)S(1)}, u32[]{:S(2)}, u32[]{:S(2)}) collective-permute-start(bf16[512,512]{1,0:T(8,128)(2,1)S(1)} %copy-done), channel_id=1, source_target_pairs={{0,1},{1,0},{2,3},{3,2},{4,5},{5,4},{6,7},{7,6},{8,9},{9,8},{10,11... | collective-permute-start | bytes 1572872 | tf_op jit(solution)/shard_map/ppermute | solution.py:48
  84.4 44.8 %collective-permute-start.13 = (bf16[2,4,64,1024]{3,2,1,0:T(8,128)(2,1)}, bf16[2,4,64,1024]{3,2,1,0:T(8,128)(2,1)S(1)}, u32[]{:S(2)}, u32[]{:S(2)}) collective-permute-start(bf16[2,4,64,1024]{3,2,1,0:T(8,128)(2,1)} %get-tuple-element.71), channel_id=1, source_target_pairs={{0,8},{8,0},{16,24},{24,16},{1,9},{9,1},{17,25},{25,17},{2,10},{10... | collective-permute-start | bytes 3145736 | tf_op jit(solution)/shard_map/ppermute | solution.py:29
  89.0 38.5 %collective-permute-start.46 = (bf16[6,128,512]{2,1,0:T(8,128)(2,1)S(1)}, bf16[6,128,512]{2,1,0:T(8,128)(2,1)S(1)}, u32[]{:S(2)}, u32[]{:S(2)}) collective-permute-start(bf16[6,128,512]{2,1,0:T(8,128)(2,1)S(1)} %copy-done.54), channel_id=1, source_target_pairs={{0,8},{8,0},{16,24},{24,16},{1,9},{9,1},{17,25},{25,17},{2,10},{10... | collective-permute-start | bytes 2359304 | tf_op jit(solution)/shard_map/ppermute | solution.py:29
  112.2 44.2 %collective-permute-start.14 = (bf16[2,4,64,1024]{3,2,1,0:T(8,128)(2,1)}, bf16[2,4,64,1024]{3,2,1,0:T(8,128)(2,1)S(1)}, u32[]{:S(2)}, u32[]{:S(2)}) collective-permute-start(bf16[2,4,64,1024]{3,2,1,0:T(8,128)(2,1)} %get-tuple-element.72), channel_id=1, source_target_pairs={{0,16},{8,24},{16,0},{24,8},{1,17},{9,25},{17,1},{25,9},{2,18},{10... | collective-permute-start | bytes 3145736 | tf_op jit(solution)/shard_map/ppermute | solution.py:29
  113.6 45.2 %collective-permute-start.15 = (bf16[2,4,64,1024]{3,2,1,0:T(8,128)(2,1)}, bf16[2,4,64,1024]{3,2,1,0:T(8,128)(2,1)S(1)}, u32[]{:S(2)}, u32[]{:S(2)}) collective-permute-start(bf16[2,4,64,1024]{3,2,1,0:T(8,128)(2,1)} %get-tuple-element.73), channel_id=1, source_target_pairs={{0,24},{8,16},{16,8},{24,0},{1,25},{9,17},{17,9},{25,1},{2,26},{10... | collective-permute-start | bytes 3145736 | tf_op jit(solution)/shard_map/ppermute | solution.py:29
  127.5 31.9 %collective-permute-start.7 = (bf16[512,512]{1,0:T(8,128)(2,1)S(1)}, bf16[512,512]{1,0:T(8,128)(2,1)S(1)}, u32[]{:S(2)}, u32[]{:S(2)}) collective-permute-start(bf16[512,512]{1,0:T(8,128)(2,1)S(1)} %collective-permute-done.3.refs_1_), channel_id=1, source_target_pairs={{0,1},{1,0},{2,3},{3,2},{4,5},{5,4},{6,7},{7,6},{8,9},{9,8},{10,11... | collective-permute-start | bytes 1572872 | tf_op jit(solution)/shard_map/ppermute | solution.py:48
  127.5 109.6 %collective-permute-start.26 = (bf16[2,6,64,1024]{3,2,1,0:T(8,128)(2,1)}, bf16[2,6,64,1024]{3,2,1,0:T(8,128)(2,1)S(1)}, u32[]{:S(2)}, u32[]{:S(2)}) collective-permute-start(bf16[2,6,64,1024]{3,2,1,0:T(8,128)(2,1)} %get-tuple-element.79), channel_id=1, source_target_pairs={{0,8},{8,0},{16,24},{24,16},{1,9},{9,1},{17,25},{25,17},{2,10},{10... | collective-permute-start | bytes 4718600 | tf_op jit(solution)/shard_map/ppermute | solution.py:29
  156.4 45.4 %collective-permute-start.48 = (bf16[6,128,512]{2,1,0:T(8,128)(2,1)}, bf16[6,128,512]{2,1,0:T(8,128)(2,1)}, u32[]{:S(2)}, u32[]{:S(2)}) collective-permute-start(bf16[6,128,512]{2,1,0:T(8,128)(2,1)} %get-tuple-element.95), channel_id=1, source_target_pairs={{0,24},{8,16},{16,8},{24,0},{1,25},{9,17},{17,9},{25,1},{2,26},{10... | collective-permute-start | bytes 2359304 | tf_op jit(solution)/shard_map/ppermute | solution.py:29
  158.8 57.3 %collective-permute-start.49 = (bf16[6,128,512]{2,1,0:T(8,128)(2,1)}, bf16[6,128,512]{2,1,0:T(8,128)(2,1)}, u32[]{:S(2)}, u32[]{:S(2)}) collective-permute-start(bf16[6,128,512]{2,1,0:T(8,128)(2,1)} %get-tuple-element.98), channel_id=1, source_target_pairs={{0,8},{8,0},{16,24},{24,16},{1,9},{9,1},{17,25},{25,17},{2,10},{10... | collective-permute-start | bytes 2359304 | tf_op jit(solution)/shard_map/ppermute | solution.py:29
  159.4 58.6 %collective-permute-start.50 = (bf16[6,128,512]{2,1,0:T(8,128)(2,1)}, bf16[6,128,512]{2,1,0:T(8,128)(2,1)}, u32[]{:S(2)}, u32[]{:S(2)}) collective-permute-start(bf16[6,128,512]{2,1,0:T(8,128)(2,1)} %get-tuple-element.99), channel_id=1, source_target_pairs={{0,16},{8,24},{16,0},{24,8},{1,17},{9,25},{17,1},{25,9},{2,18},{10... | collective-permute-start | bytes 2359304 | tf_op jit(solution)/shard_map/ppermute | solution.py:29
  162.1 102.3 %collective-permute-start.27 = (bf16[2,6,64,1024]{3,2,1,0:T(8,128)(2,1)}, bf16[2,6,64,1024]{3,2,1,0:T(8,128)(2,1)S(1)}, u32[]{:S(2)}, u32[]{:S(2)}) collective-permute-start(bf16[2,6,64,1024]{3,2,1,0:T(8,128)(2,1)} %get-tuple-element.80), channel_id=1, source_target_pairs={{0,16},{8,24},{16,0},{24,8},{1,17},{9,25},{17,1},{25,9},{2,18},{10... | collective-permute-start | bytes 4718600 | tf_op jit(solution)/shard_map/ppermute | solution.py:29
  218.0 47.8 %collective-permute-start.28 = (bf16[2,6,64,1024]{3,2,1,0:T(8,128)(2,1)}, bf16[2,6,64,1024]{3,2,1,0:T(8,128)(2,1)S(1)}, u32[]{:S(2)}, u32[]{:S(2)}) collective-permute-start(bf16[2,6,64,1024]{3,2,1,0:T(8,128)(2,1)} %get-tuple-element.81), channel_id=1, source_target_pairs={{0,24},{8,16},{16,8},{24,0},{1,25},{9,17},{17,9},{25,1},{2,26},{10... | collective-permute-start | bytes 4718600 | tf_op jit(solution)/shard_map/ppermute | solution.py:29
  220.4 69.7 %collective-permute-start.29 = (bf16[2,6,64,1024]{3,2,1,0:T(8,128)(2,1)}, bf16[2,6,64,1024]{3,2,1,0:T(8,128)(2,1)S(1)}, u32[]{:S(2)}, u32[]{:S(2)}) collective-permute-start(bf16[2,6,64,1024]{3,2,1,0:T(8,128)(2,1)} %get-tuple-element.83), channel_id=1, source_target_pairs={{0,8},{8,0},{16,24},{24,16},{1,9},{9,1},{17,25},{25,17},{2,10},{10... | collective-permute-start | bytes 4718600 | tf_op jit(solution)/shard_map/ppermute | solution.py:29
  235.4 112.7 %collective-permute-start.30 = (bf16[2,6,64,1024]{3,2,1,0:T(8,128)(2,1)}, bf16[2,6,64,1024]{3,2,1,0:T(8,128)(2,1)S(1)}, u32[]{:S(2)}, u32[]{:S(2)}) collective-permute-start(bf16[2,6,64,1024]{3,2,1,0:T(8,128)(2,1)} %get-tuple-element.84), channel_id=1, source_target_pairs={{0,16},{8,24},{16,0},{24,8},{1,17},{9,25},{17,1},{25,9},{2,18},{10... | collective-permute-start | bytes 4718600 | tf_op jit(solution)/shard_map/ppermute | solution.py:29
  237.1 111.0 %collective-permute-start.31 = (bf16[2,6,64,1024]{3,2,1,0:T(8,128)(2,1)}, bf16[2,6,64,1024]{3,2,1,0:T(8,128)(2,1)S(1)}, u32[]{:S(2)}, u32[]{:S(2)}) collective-permute-start(bf16[2,6,64,1024]{3,2,1,0:T(8,128)(2,1)} %get-tuple-element.85), channel_id=1, source_target_pairs={{0,24},{8,16},{16,8},{24,0},{1,25},{9,17},{17,9},{25,1},{2,26},{10... | collective-permute-start | bytes 4718600 | tf_op jit(solution)/shard_map/ppermute | solution.py:29
  264.3 105.9 %collective-permute-start.51 = (bf16[6,128,512]{2,1,0:T(8,128)(2,1)}, bf16[6,128,512]{2,1,0:T(8,128)(2,1)}, u32[]{:S(2)}, u32[]{:S(2)}) collective-permute-start(bf16[6,128,512]{2,1,0:T(8,128)(2,1)} %get-tuple-element.100), channel_id=1, source_target_pairs={{0,24},{8,16},{16,8},{24,0},{1,25},{9,17},{17,9},{25,1},{2,26},{10... | collective-permute-start | bytes 2359304 | tf_op jit(solution)/shard_map/ppermute | solution.py:29
  265.8 114.9 %collective-permute-start.21 = (bf16[512,320]{1,0:T(8,128)(2,1)}, bf16[512,320]{1,0:T(8,128)(2,1)S(1)}, u32[]{:S(2)}, u32[]{:S(2)}) collective-permute-start(bf16[512,320]{1,0:T(8,128)(2,1)} %get-tuple-element.77.refs_0_.refs_2_), channel_id=1, source_target_pairs={{0,6},{1,7},{2,4},{3,5},{4,2},{5,3},{6,0},{7,1},{8,14},{9,15},{10,... | collective-permute-start | bytes 983048 | tf_op jit(solution)/shard_map/ppermute | solution.py:42
  290.1 91.1 %collective-permute-start.22 = (bf16[512,320]{1,0:T(8,128)(2,1)}, bf16[512,320]{1,0:T(8,128)(2,1)S(1)}, u32[]{:S(2)}, u32[]{:S(2)}) collective-permute-start(bf16[512,320]{1,0:T(8,128)(2,1)} %get-tuple-element.77.refs_0_.refs_2_), channel_id=1, source_target_pairs={{0,1},{1,0},{2,3},{3,2},{4,5},{5,4},{6,7},{7,6},{8,9},{9,8},{10,11... | collective-permute-start | bytes 983048 | tf_op jit(solution)/shard_map/ppermute | solution.py:48
  348.1 35.0 %collective-permute-start.23 = (bf16[512,320]{1,0:T(8,128)(2,1)S(1)}, bf16[512,320]{1,0:T(8,128)(2,1)S(1)}, u32[]{:S(2)}, u32[]{:S(2)}) collective-permute-start(bf16[512,320]{1,0:T(8,128)(2,1)S(1)} %collective-permute-done.19.refs_1_.refs_3_), channel_id=1, source_target_pairs={{0,1},{1,0},{2,3},{3,2},{4,5},{5,4},{6,7},{7,6},{8,9},{9,8},{10,11... | collective-permute-start | bytes 983048 | tf_op jit(solution)/shard_map/ppermute | solution.py:48
  348.1 35.0 %collective-permute-start.24 = (bf16[512,320]{1,0:T(8,128)(2,1)S(1)}, bf16[512,320]{1,0:T(8,128)(2,1)S(1)}, u32[]{:S(2)}, u32[]{:S(2)}) collective-permute-start(bf16[512,320]{1,0:T(8,128)(2,1)S(1)} %collective-permute-done.20.refs_2_.refs_4_), channel_id=1, source_target_pairs={{0,1},{1,0},{2,3},{3,2},{4,5},{5,4},{6,7},{7,6},{8,9},{9,8},{10,11... | collective-permute-start | bytes 983048 | tf_op jit(solution)/shard_map/ppermute | solution.py:48
  381.2 31.4 %collective-permute-start.34 = (bf16[512,384]{1,0:T(8,128)(2,1)}, bf16[512,384]{1,0:T(8,128)(2,1)S(1)}, u32[]{:S(2)}, u32[]{:S(2)}) collective-permute-start(bf16[512,384]{1,0:T(8,128)(2,1)} %get-tuple-element.90.refs_2_), channel_id=1, source_target_pairs={{0,6},{1,7},{2,4},{3,5},{4,2},{5,3},{6,0},{7,1},{8,14},{9,15},{10,... | collective-permute-start | bytes 1179656 | tf_op jit(solution)/shard_map/ppermute | solution.py:42
  398.3 46.1 %collective-permute-start.40 = (bf16[512,384]{1,0:T(8,128)(2,1)S(1)}, bf16[512,384]{1,0:T(8,128)(2,1)}, u32[]{:S(2)}, u32[]{:S(2)}) collective-permute-start(bf16[512,384]{1,0:T(8,128)(2,1)S(1)} %copy-done.26), channel_id=1, source_target_pairs={{0,4},{1,5},{2,6},{3,7},{4,0},{5,1},{6,2},{7,3},{8,12},{9,13},{10,... | collective-permute-start | bytes 1179656 | tf_op jit(solution)/shard_map/ppermute | solution.py:42
  410.7 33.8 %collective-permute-start.41 = (bf16[512,384]{1,0:T(8,128)(2,1)S(1)}, bf16[512,384]{1,0:T(8,128)(2,1)}, u32[]{:S(2)}, u32[]{:S(2)}) collective-permute-start(bf16[512,384]{1,0:T(8,128)(2,1)S(1)} %copy-done.26), channel_id=1, source_target_pairs={{0,6},{1,7},{2,4},{3,5},{4,2},{5,3},{6,0},{7,1},{8,14},{9,15},{10,... | collective-permute-start | bytes 1179656 | tf_op jit(solution)/shard_map/ppermute | solution.py:42
  412.6 32.4 %collective-permute-start.42 = (bf16[512,384]{1,0:T(8,128)(2,1)S(1)}, bf16[512,384]{1,0:T(8,128)(2,1)S(1)}, u32[]{:S(2)}, u32[]{:S(2)}) collective-permute-start(bf16[512,384]{1,0:T(8,128)(2,1)S(1)} %copy-done.26), channel_id=1, source_target_pairs={{0,1},{1,0},{2,3},{3,2},{4,5},{5,4},{6,7},{7,6},{8,9},{9,8},{10,11... | collective-permute-start | bytes 1179656 | tf_op jit(solution)/shard_map/ppermute | solution.py:48
  412.6 32.5 %collective-permute-start.36 = (bf16[512,384]{1,0:T(8,128)(2,1)S(1)}, bf16[512,384]{1,0:T(8,128)(2,1)S(1)}, u32[]{:S(2)}, u32[]{:S(2)}) collective-permute-start(bf16[512,384]{1,0:T(8,128)(2,1)S(1)} %collective-permute-done.32.refs_3_), channel_id=1, source_target_pairs={{0,1},{1,0},{2,3},{3,2},{4,5},{5,4},{6,7},{7,6},{8,9},{9,8},{10,11... | collective-permute-start | bytes 1179656 | tf_op jit(solution)/shard_map/ppermute | solution.py:48
  415.7 33.7 %collective-permute-start.37 = (bf16[512,384]{1,0:T(8,128)(2,1)S(1)}, bf16[512,384]{1,0:T(8,128)(2,1)}, u32[]{:S(2)}, u32[]{:S(2)}) collective-permute-start(bf16[512,384]{1,0:T(8,128)(2,1)S(1)} %collective-permute-done.33.refs_4_), channel_id=1, source_target_pairs={{0,1},{1,0},{2,3},{3,2},{4,5},{5,4},{6,7},{7,6},{8,9},{9,8},{10,11... | collective-permute-start | bytes 1179656 | tf_op jit(solution)/shard_map/ppermute | solution.py:48
  456.0 33.5 %collective-permute-start.61 = (bf16[128,512]{1,0:T(8,128)(2,1)}, bf16[128,512]{1,0:T(8,128)(2,1)S(1)}, u32[]{:S(2)}, u32[]{:S(2)}) collective-permute-start(bf16[128,512]{1,0:T(8,128)(2,1)} %convert_element_type.23.refs_8_.refs_0_), channel_id=1, source_target_pairs={{0,8},{8,0},{16,24},{24,16},{1,9},{9,1},{17,25},{25,17},{2,10},{10... | collective-permute-start | bytes 393224 | tf_op jit(solution)/shard_map/ppermute | solution.py:29
  (87 other events, 2503.7 us)

commit v2 on v1

--- a/solution.py
+++ b/solution.py
@@ -56,15 +56,12 @@
 
 
 def cuts(count):
-    marks = [0] + [-(-count * num // 16) for num in (4, 10, 16)]
+    marks = [0] + [-(-count * num // 16) for num in (2, 8, 16)]
     return [(lo, hi - lo) for lo, hi in zip(marks, marks[1:]) if hi > lo]
 
 
 def down_cuts(chunks):
-    steps = [(c, *chunks[c]) for c in range(1, len(chunks))]
-    lo, count = chunks[0]
-    head = count // 2
-    return steps + [(0, *part) for part in ((lo, head), (lo + head, count - head)) if part[1]]
+    return [(c, *chunks[c]) for c in [*range(1, len(chunks)), 0]]
 
 
 TOKEN = jax.ShapeDtypeStruct((8, 128), jnp.float32)
@@ -209,22 +206,51 @@
     )(me, source, *gathered, down)
 
 
-def stack_rows_body(n, blk_ref, *refs):
-    own = refs[0].shape[0]
-    for s in range(n):
-        refs[-1][pl.ds(pl.multiple_of(blk_ref[s] * own, own), own), :] = refs[s][...]
-
-
-def stack_rows(blk, pieces, token):
+def finish_body(n, lo, count, blk_ref, *refs):
+    pieces, shared_pieces, refs = refs[:n], refs[n : 2 * n], refs[2 * n + 2 :]
+    down_out, shared_out, buf, in_sem, out_sem = refs
+    hf = pieces[0].shape[1]
+    copies = []
+    for s in range(n):
+        rows = pl.ds(pl.multiple_of(blk_ref[s] * hf, hf), hf)
+        head = buf.at[pl.ds(0, count), rows]
+        copies.append(pltpu.make_async_copy(pieces[s], head, in_sem.at[s, 0]))
+        copies.append(pltpu.make_async_copy(shared_pieces[s], buf.at[count, rows], in_sem.at[s, 1]))
+    for copy in copies:
+        copy.start()
+    for copy in copies:
+        copy.wait()
+    copies = [
+        pltpu.make_async_copy(
+            buf.at[pl.ds(0, count)], down_out.at[pl.ds(lo, count)], out_sem.at[0]
+        ),
+        pltpu.make_async_copy(buf.at[count], shared_out, out_sem.at[1]),
+    ]
+    for copy in copies:
+        copy.start()
+    for copy in copies:
+        copy.wait()
+
+
+def finish(blk, pieces, shared_pieces, down_serve, token, lo):
     n = len(pieces)
-    own, dp = pieces[0].shape
-    return pl.pallas_call(
-        functools.partial(stack_rows_body, n),
-        in_specs=[SMEM] + [VMEM] * n + [ANY],
-        out_specs=VMEM,
-        out_shape=jax.ShapeDtypeStruct((n * own, dp), pieces[0].dtype),
-        name="stack_rows",
-    )(blk, *pieces, token)
+    count, hf, dp = pieces[0].shape
+    return pl.pallas_call(
+        functools.partial(finish_body, n, lo, count),
+        in_specs=[SMEM] + [ANY] * (2 * n + 2),
+        out_specs=[ANY] * 2,
+        out_shape=[
+            jax.ShapeDtypeStruct(down_serve.shape, down_serve.dtype),
+            jax.ShapeDtypeStruct((n * hf, dp), down_serve.dtype),
+        ],
+        scratch_shapes=[
+            pltpu.VMEM((count + 1, n * hf, dp), down_serve.dtype),
+            pltpu.SemaphoreType.DMA((n, 2)),
+            pltpu.SemaphoreType.DMA((2,)),
+        ],
+        input_output_aliases={2 * n + 2: 0},
+        name="finish",
+    )(blk, *pieces, *shared_pieces, token, down_serve)
 
 
 def gu_body(n, lo, count, shared, first, *refs):
@@ -232,7 +258,7 @@
     take = lambda k: [refs.pop(0) for _ in range(k)]
     (blk_ref, x_ref, inv_ref, w_ref) = take(4)
     pieces = take(n)
-    shared_pieces = take(n) if shared else []
+    shared_pieces = [take(k) for k in shared]
     take(1 if first else 2)
     gate_out, up_out = take(2)
     shared_out = take(2) if shared else []
@@ -245,10 +271,15 @@
     incoming = []
     for s in range(n):
         here = [pltpu.make_async_copy(pieces[s], buf.at[s, :, pl.ds(0, count)], in_sem.at[s, 0])]
-        if shared:
-            here.append(
-                pltpu.make_async_copy(shared_pieces[s], buf.at[s, :, count], in_sem.at[s, 1])
-            )
+        if shared and shared[s] == 1:
+            whole = shared_pieces[s][0]
+            here.append(pltpu.make_async_copy(whole, buf.at[s, :, count], in_sem.at[s, 1]))
+        elif shared:
+            for m in range(2):
+                part = shared_pieces[s][m]
+                here.append(
+                    pltpu.make_async_copy(part, buf.at[s, m, count], in_sem.at[s, 1 + m])
+                )
         for copy in here:
             copy.start()
         incoming.append(here)
@@ -305,7 +336,8 @@
     n = len(pieces)
     hp, df = pieces[0].shape[-2:]
     rows = x.shape[1]
-    shared = bool(shared_pieces)
+    shared = tuple(len(group) for group in shared_pieces)
+    shared_pieces = [piece for group in shared_pieces for piece in group]
     tot = count + (1 if shared else 0)
     bf = jnp.bfloat16
     out_shape = [jax.ShapeDtypeStruct((n_local, hp, width), bf)] * 2
@@ -324,7 +356,7 @@
             pltpu.VMEM((n, 2, tot, hp, df), bf),
             pltpu.VMEM((rows, tot * hp), jnp.float32),
             pltpu.VMEM((rows, tot * hp), jnp.float32),
-            pltpu.SemaphoreType.DMA((n, 2)),
+            pltpu.SemaphoreType.DMA((n, 3)),
             pltpu.SemaphoreType.DMA((n, 2, 2)),
         ],
         input_output_aliases=aliases,
@@ -339,9 +371,9 @@
     gathered = take(parts)
     (acc_in,) = take(1)
     pieces = take(n)
-    if not first:
+    if not first and not last:
         take(1)
-    (down_out,) = take(1)
+    (down_out,) = [None] if last else take(1)
     results = take(n) if last else take(1)
     buf, a_buf, acc, in_sem, a_sem, out_sem = refs
     share = parts // n
@@ -362,7 +394,7 @@
     for copy in copies:
         copy.wait()
     out = []
-    for p in range(parts):
+    for p in range(0 if last else parts):
         rows = down_out.at[pl.ds(lo, count), pl.ds(p * hp, hp), :]
         out.append(pltpu.make_async_copy(buf.at[p], rows, out_sem.at[p]))
     for copy in out:
@@ -387,9 +419,9 @@
     gathered = take(parts)
     (acc_in,) = take(1)
     pieces = take(n)
-    if not first:
+    if not first and not last:
         take(1)
-    (down_out,) = take(1)
+    (down_out,) = [None] if last else take(1)
     results = take(n) if last else take(1)
     buf, in_sem, out_sem = refs
     hf = pieces[0].shape[1]
@@ -401,8 +433,9 @@
         copy.start()
     for copy in copies:
         copy.wait()
-    out = pltpu.make_async_copy(buf, down_out.at[pl.ds(lo, count)], out_sem)
-    out.start()
+    if not last:
+        out = pltpu.make_async_copy(buf, down_out.at[pl.ds(lo, count)], out_sem)
+        out.start()
     hp = buf.shape[1] // parts
     dp = buf.shape[2]
     lanes = slice(skip * hp, (skip + count) * hp)
@@ -418,7 +451,8 @@
             results[r][...] = total.astype(results[r].dtype)
         else:
             results[0][at, :] = total
-    out.wait()
+    if not last:
+        out.wait()
 
 
 def down_step(source, blk, gathered, acc, pieces, prev, lo, count, skip, n_local, last):
@@ -431,13 +465,13 @@
     share = parts // n
     first = prev is None
     bf = jnp.bfloat16
-    out_shape = [jax.ShapeDtypeStruct((n_local, hidden, dp), bf)]
     if last:
-        out_shape.append(jax.ShapeDtypeStruct((own, dp), jnp.float32))
+        out_shape = [jax.ShapeDtypeStruct((own, dp), jnp.float32)]
         out_shape += [jax.ShapeDtypeStruct((own, dp), bf)] * (n - 1)
     else:
+        out_shape = [jax.ShapeDtypeStruct((n_local, hidden, dp), bf)]
         out_shape.append(jax.ShapeDtypeStruct((rows, dp), jnp.float32))
-    args = [source, blk, *gathered, acc, *pieces] + ([] if first else [prev])
+    args = [source, blk, *gathered, acc, *pieces] + ([] if first or last else [prev])
     specs = [SMEM] * 2 + [ANY] * (len(args) - 2)
     if count * hp % 128 == 0 and skip * hp % 128 == 0 and share * hp == hf:
         kernel = down_body
@@ -460,10 +494,10 @@
     return pl.pallas_call(
         functools.partial(kernel, n, parts, lo, count, skip, first, last),
         in_specs=specs,
-        out_specs=[ANY] + [VMEM] * (len(out_shape) - 1),
+        out_specs=[VMEM] * n if last else [ANY, VMEM],
         out_shape=out_shape,
         scratch_shapes=scratch,
-        input_output_aliases={} if first else {len(args) - 1: 0},
+        input_output_aliases={} if first or last else {len(args) - 1: 0},
         compiler_params=pltpu.CompilerParams(vmem_limit_bytes=VMEM_LIMIT),
     )(*args)
 
@@ -497,7 +531,12 @@
     token_pieces = swap([tokens] * n)
 
     shared_gu = (jnp.stack([shared_gate_train, shared_up_train]) * gain).astype(bf)
-    shared_gu = swap([shared_gu] * n)
+    if n == 4:
+        near = [exchange(shared_gu, "fs", n, s) for s in (1, 2)]
+        far = [exchange(near[0][0], "fs", n, 2), exchange(near[1][1], "fs", n, 1)]
+        shared_gu = [[shared_gu], *([piece] for piece in near), far]
+    else:
+        shared_gu = [[piece] for piece in swap([shared_gu] * n)]
     table = jnp.concatenate([expert_ids.astype(jnp.float32).T, affinity.T])
     tables = swap([table] * n)
     chunks = cuts(n_local)
@@ -507,13 +546,13 @@
     for c, (lo, count) in enumerate(chunks):
         *pieces, token = prep_gu(gate_train, up_train, gain, base, lo, count, token)
         gu[c] = swap(pieces)
-        if c == 0:
+        if c == 1:
             token = packed = pack(token_pieces, token)
             x_same = gather_z(packed)
     for i, (_, lo, count) in enumerate(steps):
         *pieces, token = prep_down(down_train, base, lo, count, token)
         down[i] = swap(pieces)
-        if i == 0:
+        if i == len(steps) - 2:
             first_token = token
     own_shared_down = shared_down_train.astype(bf)
     shared_down = swap([own_shared_down] * n)
@@ -539,16 +578,20 @@
     down_serve = None
     for i, (c, lo, count) in enumerate(steps):
         last = i == len(steps) - 1
-        skip = lo - chunks[c][0]
-        down_serve, acc, *sums = down_step(
+        results = down_step(
             *(source, blk, gathered[c], acc, down[i], down_serve),
-            *(lo, count, skip, n_local, last),
+            *(lo, count, lo - chunks[c][0], n_local, last),
         )
-    shared_down_serve = stack_rows(blk, shared_down, acc)
-    sums = [acc, *sums]
+        if not last:
+            down_serve, acc = results
+    sums = list(results)
+    back = [give_back(sums[s], "fs", n, s) for s in range(1, n)]
+    down_serve, shared_down_serve = finish(
+        blk, down[len(steps) - 1], shared_down, down_serve, sums[0], steps[-1][1]
+    )
     total = sums[0]
-    for s in range(1, n):
-        total = total + give_back(sums[s], "fs", n, s).astype(jnp.float32)
+    for part in back:
+        total = total + part.astype(jnp.float32)
     return (
         total.astype(bf),
         gate_serve,

time: 502 us -> 510 us (1.016)
  waiting for transfers between devices: 288 us -> 312 us
  Pallas kernels: 112 us -> 106 us
    ppermute x33 -> x31, waiting for transfers between devices: 190 us -> 224 us  [exchange(): return lax.ppermute(x, axis, [(i, partner(i, s, n)[0]) for i in range(n)])]
    ppermute x33 -> x31, starting transfers between devices: 46.3 us -> 38.2 us  [exchange(): return lax.ppermute(x, axis, [(i, partner(i, s, n)[0]) for i in range(n)])]
    ppermute x12, waiting for transfers between devices: 93.3 us -> 85.6 us  [gather_z(): got.append(lax.ppermute(x, 'tp', pairs))]
    ppermute x12, starting transfers between devices: 29.6 us -> 36.3 us  [gather_z(): got.append(lax.ppermute(x, 'tp', pairs))]
    pallas_call x4 -> x3, Pallas kernels: 23.2 us -> 19 us  [down_step(): pl.pallas_call(functools.partial(kernel, n, parts, lo, count, skip, first...]
    pallas_call x4 -> x3, Pallas kernels: 19.3 us -> 17.9 us  [prep_down(): pl.pallas_call(functools.partial(prep_down_body, n), grid_spec=pltpu.Pref...]
  transfers between devices with their start and end apart: 64 -> 62, of which waited for: 22 -> 13; matrix products, arithmetic and copies ran while one was open for 1% -> 1% of each run, Pallas kernels for 23% -> 21%
where the time goes in v2:
time: 510 us; the launch traced here: 509 us
  waiting for transfers between devices  312 us (61%)
  Pallas kernels  106 us (21%)
  starting transfers between devices  80.4 us (16%)
  other arithmetic  5.44 us (1%)
    ppermute x31, waiting for transfers between devices, exchange(): return lax.ppermute(x, axis, [(i, partner(i, s, n)[0]) for i in range(n)])  224 us
    ppermute x12, waiting for transfers between devices, gather_z(): got.append(lax.ppermute(x, 'tp', pairs))  85.6 us
    ppermute x31, starting transfers between devices, exchange(): return lax.ppermute(x, axis, [(i, partner(i, s, n)[0]) for i in range(n)])  38.2 us
    ppermute x12, starting transfers between devices, gather_z(): got.append(lax.ppermute(x, 'tp', pairs))  36.3 us
    pallas_call x3, Pallas kernels, gu_step(): pl.pallas_call(functools.partial(gu_body, n, lo, count, shared, not prev)...  28.9 us
    pallas_call x3, Pallas kernels, prep_gu(): pl.pallas_call(functools.partial(prep_gu_body, n), grid_spec=pltpu.Prefet...  24.4 us
    pallas_call x3, Pallas kernels, down_step(): pl.pallas_call(functools.partial(kernel, n, parts, lo, count, skip, first...  19 us
    pallas_call x3, Pallas kernels, prep_down(): pl.pallas_call(functools.partial(prep_down_body, n), grid_spec=pltpu.Pref...  17.9 us
  transfers between devices with their start and end apart: 62, of which 13 were waited for; matrix products, arithmetic and copies ran while one was open for 1% of the time, Pallas kernels for 21%

profile of v2, /device:TPU:0, one launch (start us, length us, event | category | flops | bytes accessed | tf_op | source)
XLA Modules:
  0.0 509.1 jit_solution(5979651640763746271)
XLA Ops:
  0.6 4.0 collective-permute-start.2
  12.8 3.9 shard_map.153
  16.7 9.1 %shard_map.154 = (bf16[2,6,64,1024]{3,2,1,0:T(8,128)(2,1)}, bf16[2,6,64,1024]{3,2,1,0:T(8,128)(2,1)}, bf16[2,6,64,1024]{3,2,1,0:T(8,128)(2,1)}, bf16[2,6,64,1024]{3,2,1,0:T(8,128)(2,1)}, f32[8,128]{1,0:T(8,128)}) custom-call(s32[4]{0:T(128)} %get-tuple-element.113.idx_ref, f32[1,1024]{1,0:T(1,128)} %bitcast.25, f32[64,64,1024]{2,1,0:T(8,128)} %refs_3_.8, ...), custom_call_target="tpu_custom_call" | custom-call | tf_op jit(solution)/shard_map/pallas_call | solution.py:83
  32.0 2.2 collective-permute-start.15
  34.9 21.4 %collective-permute-done.19.refs_12_ = bf16[64,1024]{1,0:T(8,128)(2,1)S(1)} collective-permute-done((bf16[64,1024]{1,0:T(8,128)(2,1)S(1)}, bf16[64,1024]{1,0:T(8,128)(2,1)S(1)}, u32[]{:S(2)}, u32[]{:S(2)}) %collective-permute-start.19) | collective-permute-done | bytes 131104 | tf_op jit(solution)/shard_map/ppermute | solution.py:29
  56.9 4.3 collective-permute-done.18.refs_11_
  61.2 3.6 collective-permute-start.5
  64.8 11.4 %shard_map.155 = (bf16[2,8,64,1024]{3,2,1,0:T(8,128)(2,1)}, bf16[2,8,64,1024]{3,2,1,0:T(8,128)(2,1)}, bf16[2,8,64,1024]{3,2,1,0:T(8,128)(2,1)}, bf16[2,8,64,1024]{3,2,1,0:T(8,128)(2,1)}, f32[8,128]{1,0:T(8,128)}) custom-call(s32[4]{0:T(128)} %get-tuple-element.113.idx_ref, f32[1,1024]{1,0:T(1,128)} %bitcast.26, f32[64,64,1024]{2,1,0:T(8,128)} %refs_3_.8, ...), custom_call_target="tpu_custom_call" | custom-call | tf_op jit(solution)/shard_map/pallas_call | solution.py:83
  76.3 6.6 %shard_map.156 = (bf16[6,128,512]{2,1,0:T(8,128)(2,1)}, bf16[6,128,512]{2,1,0:T(8,128)(2,1)}, bf16[6,128,512]{2,1,0:T(8,128)(2,1)}, bf16[6,128,512]{2,1,0:T(8,128)(2,1)}, f32[8,128]{1,0:T(8,128)}) custom-call(s32[4]{0:T(128)} %get-tuple-element.113.idx_ref, f32[64,128,512]{2,1,0:T(8,128)} %refs_3_.11, f32[64,128,512]{2,1,0:T(8,128)} %refs_3_.11, ...), custom_call_target="tpu_custom_call" | custom-call | tf_op jit(solution)/shard_map/pallas_call | solution.py:109
  85.4 20.3 %collective-permute-done.4.refs_2_ = bf16[512,512]{1,0:T(8,128)(2,1)} collective-permute-done((bf16[512,512]{1,0:T(8,128)(2,1)}, bf16[512,512]{1,0:T(8,128)(2,1)}, u32[]{:S(2)}, u32[]{:S(2)}) %collective-permute-start.4) | collective-permute-done | bytes 524320 | tf_op jit(solution)/shard_map/ppermute | solution.py:42
  108.4 8.2 %shard_map.157 = (bf16[8,128,512]{2,1,0:T(8,128)(2,1)}, bf16[8,128,512]{2,1,0:T(8,128)(2,1)}, bf16[8,128,512]{2,1,0:T(8,128)(2,1)}, bf16[8,128,512]{2,1,0:T(8,128)(2,1)}, f32[8,128]{1,0:T(8,128)}) custom-call(s32[4]{0:T(128)} %get-tuple-element.113.idx_ref, f32[64,128,512]{2,1,0:T(8,128)} %refs_3_.11, f32[64,128,512]{2,1,0:T(8,128)} %refs_3_.11, ...), custom_call_target="tpu_custom_call" | custom-call | tf_op jit(solution)/shard_map/pallas_call | solution.py:109
  119.0 2.1 collective-permute-start.52
  122.5 7.4 %route.1 = (bf16[8,512,512]{2,1,0:T(8,128)(2,1)}, f32[512,1024]{1,0:T(8,128)}, f32[512,1]{1,0:T(8,128)}) custom-call(s32[1]{0:T(128)} %bitcast.8.me_ref, s32[8]{0:T(128)} %stack.64.from_ref.refs_0_, bf16[512,512]{1,0:T(8,128)(2,1)} %pack_tokens.1.refs_0_.refs_8_, bf16[512,512]{1,0:T(8,128)(2,1)} %collective-permute-done.3.refs_1_, ...), custom_call_target="tpu_custom_call" | custom-call | tf_op jit(solution)/shard_map/route/pallas_call | solution.py:167
  129.9 8.1 %shard_map.158 = (bf16[16,64,4096]{2,1,0:T(8,128)(2,1)}, bf16[16,64,4096]{2,1,0:T(8,128)(2,1)}, bf16[64,4096]{1,0:T(8,128)(2,1)}, bf16[64,4096]{1,0:T(8,128)(2,1)}, bf16[512,192]{1,0:T(8,128)(2,1)}) custom-call(s32[4]{0:T(128)} %get-tuple-element.114.refs_0_.refs_1_.blk_ref, bf16[8,512,512]{2,1,0:T(8,128)(2,1)} %get-tuple-element.62.refs_1_, ...), custom_call_target="tpu_custom_call" | custom-call | tf_op jit(solution)/shard_map/pallas_call | solution.py:350
  138.0 67.7 %collective-permute-done.49.refs_14_ = bf16[6,128,512]{2,1,0:T(8,128)(2,1)} collective-permute-done((bf16[6,128,512]{2,1,0:T(8,128)(2,1)}, bf16[6,128,512]{2,1,0:T(8,128)(2,1)}, u32[]{:S(2)}, u32[]{:S(2)}) %collective-permute-start.49) | collective-permute-done | bytes 786464 | tf_op jit(solution)/shard_map/ppermute | solution.py:29
  205.7 2.5 collective-permute-start.22
  211.0 6.2 %collective-permute-done.22.refs_3_.refs_5_ = bf16[512,192]{1,0:T(8,128)(2,1)} collective-permute-done((bf16[512,192]{1,0:T(8,128)(2,1)}, bf16[512,192]{1,0:T(8,128)(2,1)}, u32[]{:S(2)}, u32[]{:S(2)}) %collective-permute-start.22) | collective-permute-done | bytes 196640 | tf_op jit(solution)/shard_map/ppermute | solution.py:42
  217.2 9.0 %collective-permute-start.20 = (bf16[512,192]{1,0:T(8,128)(2,1)}, bf16[512,192]{1,0:T(8,128)(2,1)}, u32[]{:S(2)}, u32[]{:S(2)}) collective-permute-start(bf16[512,192]{1,0:T(8,128)(2,1)} %get-tuple-element.72.refs_0_.refs_2_), channel_id=1, source_target_pairs={{0,2},{1,3},{2,0},{3,1},{4,6},{5,7},{6,4},{7,5},{8,10},{9,11},{10,... | collective-permute-start | bytes 589832 | tf_op jit(solution)/shard_map/ppermute | solution.py:42
  226.2 4.6 collective-permute-done.21.refs_2_.refs_4_
  232.8 3.5 collective-permute-done.20.refs_1_.refs_3_
  238.7 130.7 %collective-permute-done.31.refs_6_ = bf16[2,6,64,1024]{3,2,1,0:T(8,128)(2,1)} collective-permute-done((bf16[2,6,64,1024]{3,2,1,0:T(8,128)(2,1)}, bf16[2,6,64,1024]{3,2,1,0:T(8,128)(2,1)}, u32[]{:S(2)}, u32[]{:S(2)}) %collective-permute-start.31) | collective-permute-done | bytes 1572896 | tf_op jit(solution)/shard_map/ppermute | solution.py:29
  369.9 10.1 %shard_map.159 = (bf16[16,64,4096]{2,1,0:T(8,128)(2,1)}, bf16[16,64,4096]{2,1,0:T(8,128)(2,1)}, bf16[512,384]{1,0:T(8,128)(2,1)}) custom-call(s32[4]{0:T(128)} %get-tuple-element.114.refs_0_.refs_1_.blk_ref, bf16[8,512,512]{2,1,0:T(8,128)(2,1)} %get-tuple-element.62.refs_1_, ...), custom_call_target="tpu_custom_call", output_to_operand_aliasing={{0}: (8, {}), {1}: (9, {})} | custom-call | tf_op jit(solution)/shard_map/pallas_call | solution.py:350
  385.0 10.7 %shard_map.160 = (bf16[16,64,4096]{2,1,0:T(8,128)(2,1)}, bf16[16,64,4096]{2,1,0:T(8,128)(2,1)}, bf16[512,512]{1,0:T(8,128)(2,1)}) custom-call(s32[4]{0:T(128)} %get-tuple-element.114.refs_0_.refs_1_.blk_ref, bf16[8,512,512]{2,1,0:T(8,128)(2,1)} %get-tuple-element.62.refs_1_, ...), custom_call_target="tpu_custom_call", output_to_operand_aliasing={{0}: (8, {}), {1}: (9, {})} | custom-call | tf_op jit(solution)/shard_map/pallas_call | solution.py:350
  397.1 14.4 %collective-permute-start.34 = (bf16[512,512]{1,0:T(8,128)(2,1)}, bf16[512,512]{1,0:T(8,128)(2,1)S(1)}, u32[]{:S(2)}, u32[]{:S(2)}) collective-permute-start(bf16[512,512]{1,0:T(8,128)(2,1)} %get-tuple-element.85.refs_2_), channel_id=1, source_target_pairs={{0,4},{1,5},{2,6},{3,7},{4,0},{5,1},{6,2},{7,3},{8,12},{9,13},{10,... | collective-permute-start | bytes 1572872 | tf_op jit(solution)/shard_map/ppermute | solution.py:42
  411.6 29.5 %collective-permute-done.41.refs_4_ = bf16[512,384]{1,0:T(8,128)(2,1)} collective-permute-done((bf16[512,384]{1,0:T(8,128)(2,1)}, bf16[512,384]{1,0:T(8,128)(2,1)}, u32[]{:S(2)}, u32[]{:S(2)}) %collective-permute-start.41) | collective-permute-done | bytes 393248 | tf_op jit(solution)/shard_map/ppermute | solution.py:42
  443.2 19.5 %collective-permute-done.34.refs_4_ = bf16[512,512]{1,0:T(8,128)(2,1)S(1)} collective-permute-done((bf16[512,512]{1,0:T(8,128)(2,1)}, bf16[512,512]{1,0:T(8,128)(2,1)S(1)}, u32[]{:S(2)}, u32[]{:S(2)}) %collective-permute-start.34) | collective-permute-done | bytes 524320 | tf_op jit(solution)/shard_map/ppermute | solution.py:42
  464.7 3.0 shard_map.163
  474.8 3.2 shared_down.1.refs_10_
  478.0 6.8 %shard_map.161 = (bf16[16,512,512]{2,1,0:T(8,128)(2,1)}, f32[512,512]{1,0:T(8,128)}) custom-call(s32[8]{0:T(128)} %stack.64.from_ref.refs_0_, s32[4]{0:T(128)} %get-tuple-element.114.refs_0_.refs_1_.blk_ref, bf16[512,384]{1,0:T(8,128)(2,1)} %get-tuple-element.86.refs_2_, bf16[512,384]{1,0:T(8,128)(2,1)} %collective-permute-done.40.refs_3_, ...), custom_call_target="tpu_custom_call" | custom-call | tf_op jit(solution)/shard_map/pallas_call | solution.py:494
  485.6 7.9 %shard_map.162 = (bf16[16,512,512]{2,1,0:T(8,128)(2,1)}, f32[512,512]{1,0:T(8,128)}) custom-call(s32[8]{0:T(128)} %stack.64.from_ref.refs_0_, s32[4]{0:T(128)} %get-tuple-element.114.refs_0_.refs_1_.blk_ref, bf16[512,512]{1,0:T(8,128)(2,1)} %get-tuple-element.85.refs_2_, bf16[512,512]{1,0:T(8,128)(2,1)} %copy-done.21, ...), custom_call_target="tpu_custom_call", output_to_operand_aliasing={{0}: (15, {})} | custom-call | tf_op jit(solution)/shard_map/pallas_call | solution.py:494
  495.4 4.3 shard_map.164
  504.0 3.4 finish.1
  (199 shorter events, 58.3 us)
Async XLA Ops:
  6.3 24.8 %collective-permute-start.17 = (bf16[2,64,1024]{2,1,0:T(8,128)(2,1)S(1)}, bf16[2,64,1024]{2,1,0:T(8,128)(2,1)S(1)}, u32[]{:S(2)}, u32[]{:S(2)}) collective-permute-start(bf16[2,64,1024]{2,1,0:T(8,128)(2,1)S(1)} %fusion.refs_8_), channel_id=1, source_target_pairs={{0,16},{8,24},{16,0},{24,8},{1,17},{9,25},{17,1},{25,9},{2,18},{10... | collective-permute-start | bytes 786440 | tf_op jit(solution)/shard_map/ppermute | solution.py:29
  8.3 25.8 %collective-permute-start.16 = (bf16[2,64,1024]{2,1,0:T(8,128)(2,1)S(1)}, bf16[2,64,1024]{2,1,0:T(8,128)(2,1)S(1)}, u32[]{:S(2)}, u32[]{:S(2)}) collective-permute-start(bf16[2,64,1024]{2,1,0:T(8,128)(2,1)S(1)} %fusion.refs_8_), channel_id=1, source_target_pairs={{0,8},{8,0},{16,24},{24,16},{1,9},{9,1},{17,25},{25,17},{2,10},{10... | collective-permute-start | bytes 786440 | tf_op jit(solution)/shard_map/ppermute | solution.py:29
  30.6 34.3 %collective-permute-start.13 = (bf16[2,2,64,1024]{3,2,1,0:T(8,128)(2,1)}, bf16[2,2,64,1024]{3,2,1,0:T(8,128)(2,1)S(1)}, u32[]{:S(2)}, u32[]{:S(2)}) collective-permute-start(bf16[2,2,64,1024]{3,2,1,0:T(8,128)(2,1)} %get-tuple-element.66), channel_id=1, source_target_pairs={{0,8},{8,0},{16,24},{24,16},{1,9},{9,1},{17,25},{25,17},{2,10},{10... | collective-permute-start | bytes 1572872 | tf_op jit(solution)/shard_map/ppermute | solution.py:29
  31.2 51.8 %collective-permute-start.14 = (bf16[2,2,64,1024]{3,2,1,0:T(8,128)(2,1)}, bf16[2,2,64,1024]{3,2,1,0:T(8,128)(2,1)S(1)}, u32[]{:S(2)}, u32[]{:S(2)}) collective-permute-start(bf16[2,2,64,1024]{3,2,1,0:T(8,128)(2,1)} %get-tuple-element.67), channel_id=1, source_target_pairs={{0,16},{8,24},{16,0},{24,8},{1,17},{9,25},{17,1},{25,9},{2,18},{10... | collective-permute-start | bytes 1572872 | tf_op jit(solution)/shard_map/ppermute | solution.py:29
  32.0 52.0 %collective-permute-start.15 = (bf16[2,2,64,1024]{3,2,1,0:T(8,128)(2,1)S(1)}, bf16[2,2,64,1024]{3,2,1,0:T(8,128)(2,1)S(1)}, u32[]{:S(2)}, u32[]{:S(2)}) collective-permute-start(bf16[2,2,64,1024]{3,2,1,0:T(8,128)(2,1)S(1)} %copy-done.40), channel_id=1, source_target_pairs={{0,24},{8,16},{16,8},{24,0},{1,25},{9,17},{17,9},{25,1},{2,26},{10... | collective-permute-start | bytes 1572872 | tf_op jit(solution)/shard_map/ppermute | solution.py:29
  34.2 50.7 %collective-permute-start.6 = (bf16[512,512]{1,0:T(8,128)(2,1)}, bf16[512,512]{1,0:T(8,128)(2,1)S(1)}, u32[]{:S(2)}, u32[]{:S(2)}) collective-permute-start(bf16[512,512]{1,0:T(8,128)(2,1)} %pack_tokens.1.refs_0_.refs_8_), channel_id=1, source_target_pairs={{0,1},{1,0},{2,3},{3,2},{4,5},{5,4},{6,7},{7,6},{8,9},{9,8},{10,11... | collective-permute-start | bytes 1572872 | tf_op jit(solution)/shard_map/ppermute | solution.py:48
  61.2 24.2 %collective-permute-start.5 = (bf16[512,512]{1,0:T(8,128)(2,1)}, bf16[512,512]{1,0:T(8,128)(2,1)}, u32[]{:S(2)}, u32[]{:S(2)}) collective-permute-start(bf16[512,512]{1,0:T(8,128)(2,1)} %pack_tokens.1.refs_0_.refs_8_), channel_id=1, source_target_pairs={{0,6},{1,7},{2,4},{3,5},{4,2},{5,3},{6,0},{7,1},{8,14},{9,15},{10,... | collective-permute-start | bytes 1572872 | tf_op jit(solution)/shard_map/ppermute | solution.py:42
  64.8 40.8 %collective-permute-start.4 = (bf16[512,512]{1,0:T(8,128)(2,1)}, bf16[512,512]{1,0:T(8,128)(2,1)}, u32[]{:S(2)}, u32[]{:S(2)}) collective-permute-start(bf16[512,512]{1,0:T(8,128)(2,1)} %pack_tokens.1.refs_0_.refs_8_), channel_id=1, source_target_pairs={{0,4},{1,5},{2,6},{3,7},{4,0},{5,1},{6,2},{7,3},{8,12},{9,13},{10,... | collective-permute-start | bytes 1572872 | tf_op jit(solution)/shard_map/ppermute | solution.py:42
  84.8 31.8 %collective-permute-start.48 = (bf16[6,128,512]{2,1,0:T(8,128)(2,1)}, bf16[6,128,512]{2,1,0:T(8,128)(2,1)S(1)}, u32[]{:S(2)}, u32[]{:S(2)}) collective-permute-start(bf16[6,128,512]{2,1,0:T(8,128)(2,1)} %get-tuple-element.89), channel_id=1, source_target_pairs={{0,16},{8,24},{16,0},{24,8},{1,17},{9,25},{17,1},{25,9},{2,18},{10... | collective-permute-start | bytes 2359304 | tf_op jit(solution)/shard_map/ppermute | solution.py:29
  85.4 32.8 %collective-permute-start.9 = (bf16[512,512]{1,0:T(8,128)(2,1)}, bf16[512,512]{1,0:T(8,128)(2,1)}, u32[]{:S(2)}, u32[]{:S(2)}) collective-permute-start(bf16[512,512]{1,0:T(8,128)(2,1)} %collective-permute-done.5.refs_3_), channel_id=1, source_target_pairs={{0,1},{1,0},{2,3},{3,2},{4,5},{5,4},{6,7},{7,6},{8,9},{9,8},{10,11... | collective-permute-start | bytes 1572872 | tf_op jit(solution)/shard_map/ppermute | solution.py:48
  107.1 130.5 %collective-permute-start.30 = (bf16[2,6,64,1024]{3,2,1,0:T(8,128)(2,1)}, bf16[2,6,64,1024]{3,2,1,0:T(8,128)(2,1)S(1)}, u32[]{:S(2)}, u32[]{:S(2)}) collective-permute-start(bf16[2,6,64,1024]{3,2,1,0:T(8,128)(2,1)} %get-tuple-element.78), channel_id=1, source_target_pairs={{0,8},{8,0},{16,24},{24,16},{1,9},{9,1},{17,25},{25,17},{2,10},{10... | collective-permute-start | bytes 4718600 | tf_op jit(solution)/shard_map/ppermute | solution.py:29
  117.5 88.1 %collective-permute-start.50 = (bf16[8,128,512]{2,1,0:T(8,128)(2,1)}, bf16[8,128,512]{2,1,0:T(8,128)(2,1)S(1)}, u32[]{:S(2)}, u32[]{:S(2)}) collective-permute-start(bf16[8,128,512]{2,1,0:T(8,128)(2,1)} %get-tuple-element.93), channel_id=1, source_target_pairs={{0,8},{8,0},{16,24},{24,16},{1,9},{9,1},{17,25},{25,17},{2,10},{10... | collective-permute-start | bytes 3145736 | tf_op jit(solution)/shard_map/ppermute | solution.py:29
  118.3 90.0 %collective-permute-start.51 = (bf16[8,128,512]{2,1,0:T(8,128)(2,1)}, bf16[8,128,512]{2,1,0:T(8,128)(2,1)}, u32[]{:S(2)}, u32[]{:S(2)}) collective-permute-start(bf16[8,128,512]{2,1,0:T(8,128)(2,1)} %get-tuple-element.94), channel_id=1, source_target_pairs={{0,16},{8,24},{16,0},{24,8},{1,17},{9,25},{17,1},{25,9},{2,18},{10... | collective-permute-start | bytes 3145736 | tf_op jit(solution)/shard_map/ppermute | solution.py:29
  119.0 89.3 %collective-permute-start.52 = (bf16[8,128,512]{2,1,0:T(8,128)(2,1)}, bf16[8,128,512]{2,1,0:T(8,128)(2,1)}, u32[]{:S(2)}, u32[]{:S(2)}) collective-permute-start(bf16[8,128,512]{2,1,0:T(8,128)(2,1)} %get-tuple-element.95), channel_id=1, source_target_pairs={{0,24},{8,16},{16,8},{24,0},{1,25},{9,17},{17,9},{25,1},{2,26},{10... | collective-permute-start | bytes 3145736 | tf_op jit(solution)/shard_map/ppermute | solution.py:29
  121.0 84.6 %collective-permute-start.49 = (bf16[6,128,512]{2,1,0:T(8,128)(2,1)}, bf16[6,128,512]{2,1,0:T(8,128)(2,1)}, u32[]{:S(2)}, u32[]{:S(2)}) collective-permute-start(bf16[6,128,512]{2,1,0:T(8,128)(2,1)} %get-tuple-element.90), channel_id=1, source_target_pairs={{0,24},{8,16},{16,8},{24,0},{1,25},{9,17},{17,9},{25,1},{2,26},{10... | collective-permute-start | bytes 2359304 | tf_op jit(solution)/shard_map/ppermute | solution.py:29
  208.3 173.2 %collective-permute-start.27 = (bf16[2,8,64,1024]{3,2,1,0:T(8,128)(2,1)}, bf16[2,8,64,1024]{3,2,1,0:T(8,128)(2,1)S(1)}, u32[]{:S(2)}, u32[]{:S(2)}) collective-permute-start(bf16[2,8,64,1024]{3,2,1,0:T(8,128)(2,1)} %get-tuple-element.74), channel_id=1, source_target_pairs={{0,8},{8,0},{16,24},{24,16},{1,9},{9,1},{17,25},{25,17},{2,10},{10... | collective-permute-start | bytes 6291464 | tf_op jit(solution)/shard_map/ppermute | solution.py:29
  209.3 172.7 %collective-permute-start.28 = (bf16[2,8,64,1024]{3,2,1,0:T(8,128)(2,1)}, bf16[2,8,64,1024]{3,2,1,0:T(8,128)(2,1)}, u32[]{:S(2)}, u32[]{:S(2)}) collective-permute-start(bf16[2,8,64,1024]{3,2,1,0:T(8,128)(2,1)} %get-tuple-element.75), channel_id=1, source_target_pairs={{0,16},{8,24},{16,0},{24,8},{1,17},{9,25},{17,1},{25,9},{2,18},{10... | collective-permute-start | bytes 6291464 | tf_op jit(solution)/shard_map/ppermute | solution.py:29
  230.8 152.9 %collective-permute-start.29 = (bf16[2,8,64,1024]{3,2,1,0:T(8,128)(2,1)}, bf16[2,8,64,1024]{3,2,1,0:T(8,128)(2,1)}, u32[]{:S(2)}, u32[]{:S(2)}) collective-permute-start(bf16[2,8,64,1024]{3,2,1,0:T(8,128)(2,1)} %get-tuple-element.76), channel_id=1, source_target_pairs={{0,24},{8,16},{16,8},{24,0},{1,25},{9,17},{17,9},{25,1},{2,26},{10... | collective-permute-start | bytes 6291464 | tf_op jit(solution)/shard_map/ppermute | solution.py:29
  236.3 133.1 %collective-permute-start.31 = (bf16[2,6,64,1024]{3,2,1,0:T(8,128)(2,1)}, bf16[2,6,64,1024]{3,2,1,0:T(8,128)(2,1)}, u32[]{:S(2)}, u32[]{:S(2)}) collective-permute-start(bf16[2,6,64,1024]{3,2,1,0:T(8,128)(2,1)} %get-tuple-element.79), channel_id=1, source_target_pairs={{0,16},{8,24},{16,0},{24,8},{1,17},{9,25},{17,1},{25,9},{2,18},{10... | collective-permute-start | bytes 4718600 | tf_op jit(solution)/shard_map/ppermute | solution.py:29
  237.6 131.8 %collective-permute-start.32 = (bf16[2,6,64,1024]{3,2,1,0:T(8,128)(2,1)}, bf16[2,6,64,1024]{3,2,1,0:T(8,128)(2,1)}, u32[]{:S(2)}, u32[]{:S(2)}) collective-permute-start(bf16[2,6,64,1024]{3,2,1,0:T(8,128)(2,1)} %get-tuple-element.80), channel_id=1, source_target_pairs={{0,24},{8,16},{16,8},{24,0},{1,25},{9,17},{17,9},{25,1},{2,26},{10... | collective-permute-start | bytes 4718600 | tf_op jit(solution)/shard_map/ppermute | solution.py:29
  382.0 59.1 %collective-permute-start.41 = (bf16[512,384]{1,0:T(8,128)(2,1)}, bf16[512,384]{1,0:T(8,128)(2,1)}, u32[]{:S(2)}, u32[]{:S(2)}) collective-permute-start(bf16[512,384]{1,0:T(8,128)(2,1)} %get-tuple-element.86.refs_2_), channel_id=1, source_target_pairs={{0,4},{1,5},{2,6},{3,7},{4,0},{5,1},{6,2},{7,3},{8,12},{9,13},{10,... | collective-permute-start | bytes 1179656 | tf_op jit(solution)/shard_map/ppermute | solution.py:42
  383.6 57.5 %collective-permute-start.40 = (bf16[512,384]{1,0:T(8,128)(2,1)}, bf16[512,384]{1,0:T(8,128)(2,1)}, u32[]{:S(2)}, u32[]{:S(2)}) collective-permute-start(bf16[512,384]{1,0:T(8,128)(2,1)} %get-tuple-element.86.refs_2_), channel_id=1, source_target_pairs={{0,2},{1,3},{2,0},{3,1},{4,6},{5,7},{6,4},{7,5},{8,10},{9,11},{10,... | collective-permute-start | bytes 1179656 | tf_op jit(solution)/shard_map/ppermute | solution.py:42
  395.7 46.0 %collective-permute-start.35 = (bf16[512,512]{1,0:T(8,128)(2,1)}, bf16[512,512]{1,0:T(8,128)(2,1)S(1)}, u32[]{:S(2)}, u32[]{:S(2)}) collective-permute-start(bf16[512,512]{1,0:T(8,128)(2,1)} %get-tuple-element.85.refs_2_), channel_id=1, source_target_pairs={{0,6},{1,7},{2,4},{3,5},{4,2},{5,3},{6,0},{7,1},{8,14},{9,15},{10,... | collective-permute-start | bytes 1572872 | tf_op jit(solution)/shard_map/ppermute | solution.py:42
  397.1 44.0 %collective-permute-start.46 = (bf16[512,384]{1,0:T(8,128)(2,1)S(1)}, bf16[512,384]{1,0:T(8,128)(2,1)S(1)}, u32[]{:S(2)}, u32[]{:S(2)}) collective-permute-start(bf16[512,384]{1,0:T(8,128)(2,1)S(1)} %collective-permute-done.42.refs_5_), channel_id=1, source_target_pairs={{0,1},{1,0},{2,3},{3,2},{4,5},{5,4},{6,7},{7,6},{8,9},{9,8},{10,11... | collective-permute-start | bytes 1179656 | tf_op jit(solution)/shard_map/ppermute | solution.py:48
  397.1 65.5 %collective-permute-start.34 = (bf16[512,512]{1,0:T(8,128)(2,1)}, bf16[512,512]{1,0:T(8,128)(2,1)S(1)}, u32[]{:S(2)}, u32[]{:S(2)}) collective-permute-start(bf16[512,512]{1,0:T(8,128)(2,1)} %get-tuple-element.85.refs_2_), channel_id=1, source_target_pairs={{0,4},{1,5},{2,6},{3,7},{4,0},{5,1},{6,2},{7,3},{8,12},{9,13},{10,... | collective-permute-start | bytes 1572872 | tf_op jit(solution)/shard_map/ppermute | solution.py:42
  441.1 27.8 %collective-permute-start.36 = (bf16[512,512]{1,0:T(8,128)(2,1)}, bf16[512,512]{1,0:T(8,128)(2,1)S(1)}, u32[]{:S(2)}, u32[]{:S(2)}) collective-permute-start(bf16[512,512]{1,0:T(8,128)(2,1)} %get-tuple-element.85.refs_2_), channel_id=1, source_target_pairs={{0,1},{1,0},{2,3},{3,2},{4,5},{5,4},{6,7},{7,6},{8,9},{9,8},{10,11... | collective-permute-start | bytes 1572872 | tf_op jit(solution)/shard_map/ppermute | solution.py:48
  441.7 28.5 %collective-permute-start.39 = (bf16[512,512]{1,0:T(8,128)(2,1)S(1)}, bf16[512,512]{1,0:T(8,128)(2,1)S(1)}, u32[]{:S(2)}, u32[]{:S(2)}) collective-permute-start(bf16[512,512]{1,0:T(8,128)(2,1)S(1)} %collective-permute-done.35.refs_5_), channel_id=1, source_target_pairs={{0,1},{1,0},{2,3},{3,2},{4,5},{5,4},{6,7},{7,6},{8,9},{9,8},{10,11... | collective-permute-start | bytes 1572872 | tf_op jit(solution)/shard_map/ppermute | solution.py:48
  443.0 24.7 %collective-permute-start.44 = (bf16[512,384]{1,0:T(8,128)(2,1)}, bf16[512,384]{1,0:T(8,128)(2,1)}, u32[]{:S(2)}, u32[]{:S(2)}) collective-permute-start(bf16[512,384]{1,0:T(8,128)(2,1)} %collective-permute-done.40.refs_3_), channel_id=1, source_target_pairs={{0,1},{1,0},{2,3},{3,2},{4,5},{5,4},{6,7},{7,6},{8,9},{9,8},{10,11... | collective-permute-start | bytes 1179656 | tf_op jit(solution)/shard_map/ppermute | solution.py:48
  467.8 25.8 %collective-permute-start.53 = (bf16[2,128,512]{2,1,0:T(8,128)(2,1)}, bf16[2,128,512]{2,1,0:T(8,128)(2,1)S(1)}, u32[]{:S(2)}, u32[]{:S(2)}) collective-permute-start(bf16[2,128,512]{2,1,0:T(8,128)(2,1)} %get-tuple-element.99), channel_id=1, source_target_pairs={{0,8},{8,0},{16,24},{24,16},{1,9},{9,1},{17,25},{25,17},{2,10},{10... | collective-permute-start | bytes 786440 | tf_op jit(solution)/shard_map/ppermute | solution.py:29
  468.9 25.7 %collective-permute-start.54 = (bf16[2,128,512]{2,1,0:T(8,128)(2,1)}, bf16[2,128,512]{2,1,0:T(8,128)(2,1)S(1)}, u32[]{:S(2)}, u32[]{:S(2)}) collective-permute-start(bf16[2,128,512]{2,1,0:T(8,128)(2,1)} %get-tuple-element.100), channel_id=1, source_target_pairs={{0,16},{8,24},{16,0},{24,8},{1,17},{9,25},{17,1},{25,9},{2,18},{10... | collective-permute-start | bytes 786440 | tf_op jit(solution)/shard_map/ppermute | solution.py:29
  470.2 24.4 %collective-permute-start.55 = (bf16[2,128,512]{2,1,0:T(8,128)(2,1)}, bf16[2,128,512]{2,1,0:T(8,128)(2,1)S(1)}, u32[]{:S(2)}, u32[]{:S(2)}) collective-permute-start(bf16[2,128,512]{2,1,0:T(8,128)(2,1)} %get-tuple-element.101), channel_id=1, source_target_pairs={{0,24},{8,16},{16,8},{24,0},{1,25},{9,17},{17,9},{25,1},{2,26},{10... | collective-permute-start | bytes 786440 | tf_op jit(solution)/shard_map/ppermute | solution.py:29
  473.0 29.2 %collective-permute-start.61 = (bf16[128,512]{1,0:T(8,128)(2,1)}, bf16[128,512]{1,0:T(8,128)(2,1)S(1)}, u32[]{:S(2)}, u32[]{:S(2)}) collective-permute-start(bf16[128,512]{1,0:T(8,128)(2,1)} %convert_element_type.23.refs_8_.refs_4_), channel_id=1, source_target_pairs={{0,24},{8,16},{16,8},{24,0},{1,25},{9,17},{17,9},{25,1},{2,26},{10... | collective-permute-start | bytes 393224 | tf_op jit(solution)/shard_map/ppermute | solution.py:29
  (71 other events, 1386.7 us)

commit v3 on v2

--- a/solution.py
+++ b/solution.py
@@ -210,25 +210,22 @@
     pieces, shared_pieces, refs = refs[:n], refs[n : 2 * n], refs[2 * n + 2 :]
     down_out, shared_out, buf, in_sem, out_sem = refs
     hf = pieces[0].shape[1]
-    copies = []
+    arriving, leaving = [], []
     for s in range(n):
         rows = pl.ds(pl.multiple_of(blk_ref[s] * hf, hf), hf)
-        head = buf.at[pl.ds(0, count), rows]
-        copies.append(pltpu.make_async_copy(pieces[s], head, in_sem.at[s, 0]))
-        copies.append(pltpu.make_async_copy(shared_pieces[s], buf.at[count, rows], in_sem.at[s, 1]))
-    for copy in copies:
+        moves = [
+            (pieces[s], buf.at[pl.ds(0, count), rows], down_out.at[pl.ds(lo, count), rows]),
+            (shared_pieces[s], buf.at[count, rows], shared_out.at[rows]),
+        ]
+        for m, (source, stage, target) in enumerate(moves):
+            arriving.append(pltpu.make_async_copy(source, stage, in_sem.at[s, m]))
+            leaving.append(pltpu.make_async_copy(stage, target, out_sem.at[s, m]))
+    for copy in arriving:
         copy.start()
-    for copy in copies:
+    for copy, onward in zip(arriving, leaving):
         copy.wait()
-    copies = [
-        pltpu.make_async_copy(
-            buf.at[pl.ds(0, count)], down_out.at[pl.ds(lo, count)], out_sem.at[0]
-        ),
-        pltpu.make_async_copy(buf.at[count], shared_out, out_sem.at[1]),
-    ]
-    for copy in copies:
-        copy.start()
-    for copy in copies:
+        onward.start()
+    for copy in leaving:
         copy.wait()
 
 
@@ -246,7 +243,7 @@
         scratch_shapes=[
             pltpu.VMEM((count + 1, n * hf, dp), down_serve.dtype),
             pltpu.SemaphoreType.DMA((n, 2)),
-            pltpu.SemaphoreType.DMA((2,)),
+            pltpu.SemaphoreType.DMA((n, 2)),
         ],
         input_output_aliases={2 * n + 2: 0},
         name="finish",

time: 510 us -> 510 us (level)
  transfers between devices with their start and end apart: 62 -> 62, of which waited for: 13 -> 14; matrix products, arithmetic and copies ran while one was open for 1% -> 1% of each run, Pallas kernels for 21% -> 21%
where the time goes in v3:
time: 510 us; the launch traced here: 509 us
  waiting for transfers between devices  312 us (61%)
  Pallas kernels  106 us (21%)
  starting transfers between devices  80.4 us (16%)
  other arithmetic  5.44 us (1%)
    ppermute x31, waiting for transfers between devices, exchange(): return lax.ppermute(x, axis, [(i, partner(i, s, n)[0]) for i in range(n)])  224 us
    ppermute x12, waiting for transfers between devices, gather_z(): got.append(lax.ppermute(x, 'tp', pairs))  85.6 us
    ppermute x31, starting transfers between devices, exchange(): return lax.ppermute(x, axis, [(i, partner(i, s, n)[0]) for i in range(n)])  38.2 us
    ppermute x12, starting transfers between devices, gather_z(): got.append(lax.ppermute(x, 'tp', pairs))  36.3 us
    pallas_call x3, Pallas kernels, gu_step(): pl.pallas_call(functools.partial(gu_body, n, lo, count, shared, not prev)...  28.9 us
    pallas_call x3, Pallas kernels, prep_gu(): pl.pallas_call(functools.partial(prep_gu_body, n), grid_spec=pltpu.Prefet...  24.4 us
    pallas_call x3, Pallas kernels, down_step(): pl.pallas_call(functools.partial(kernel, n, parts, lo, count, skip, first...  19 us
    pallas_call x3, Pallas kernels, prep_down(): pl.pallas_call(functools.partial(prep_down_body, n), grid_spec=pltpu.Pref...  17.9 us
  transfers between devices with their start and end apart: 62, of which 14 were waited for; matrix products, arithmetic and copies ran while one was open for 1% of the time, Pallas kernels for 21%

profile of v3, /device:TPU:0, one launch (start us, length us, event | category | flops | bytes accessed | tf_op | source)
XLA Modules:
  0.0 509.1 jit_solution(16684993028030844383)
XLA Ops:
  0.6 4.0 collective-permute-start.2
  12.8 3.9 shard_map.153
  16.7 9.1 %shard_map.154 = (bf16[2,6,64,1024]{3,2,1,0:T(8,128)(2,1)}, bf16[2,6,64,1024]{3,2,1,0:T(8,128)(2,1)}, bf16[2,6,64,1024]{3,2,1,0:T(8,128)(2,1)}, bf16[2,6,64,1024]{3,2,1,0:T(8,128)(2,1)}, f32[8,128]{1,0:T(8,128)}) custom-call(s32[4]{0:T(128)} %get-tuple-element.113.idx_ref, f32[1,1024]{1,0:T(1,128)} %bitcast.25, f32[64,64,1024]{2,1,0:T(8,128)} %refs_3_.8, ...), custom_call_target="tpu_custom_call" | custom-call | tf_op jit(solution)/shard_map/pallas_call | solution.py:83
  32.0 2.2 collective-permute-start.15
  34.9 21.4 %collective-permute-done.19.refs_12_ = bf16[64,1024]{1,0:T(8,128)(2,1)S(1)} collective-permute-done((bf16[64,1024]{1,0:T(8,128)(2,1)S(1)}, bf16[64,1024]{1,0:T(8,128)(2,1)S(1)}, u32[]{:S(2)}, u32[]{:S(2)}) %collective-permute-start.19) | collective-permute-done | bytes 131104 | tf_op jit(solution)/shard_map/ppermute | solution.py:29
  56.9 4.3 collective-permute-done.18.refs_11_
  61.2 3.6 collective-permute-start.5
  64.8 11.4 %shard_map.155 = (bf16[2,8,64,1024]{3,2,1,0:T(8,128)(2,1)}, bf16[2,8,64,1024]{3,2,1,0:T(8,128)(2,1)}, bf16[2,8,64,1024]{3,2,1,0:T(8,128)(2,1)}, bf16[2,8,64,1024]{3,2,1,0:T(8,128)(2,1)}, f32[8,128]{1,0:T(8,128)}) custom-call(s32[4]{0:T(128)} %get-tuple-element.113.idx_ref, f32[1,1024]{1,0:T(1,128)} %bitcast.26, f32[64,64,1024]{2,1,0:T(8,128)} %refs_3_.8, ...), custom_call_target="tpu_custom_call" | custom-call | tf_op jit(solution)/shard_map/pallas_call | solution.py:83
  76.3 6.6 %shard_map.156 = (bf16[6,128,512]{2,1,0:T(8,128)(2,1)}, bf16[6,128,512]{2,1,0:T(8,128)(2,1)}, bf16[6,128,512]{2,1,0:T(8,128)(2,1)}, bf16[6,128,512]{2,1,0:T(8,128)(2,1)}, f32[8,128]{1,0:T(8,128)}) custom-call(s32[4]{0:T(128)} %get-tuple-element.113.idx_ref, f32[64,128,512]{2,1,0:T(8,128)} %refs_3_.11, f32[64,128,512]{2,1,0:T(8,128)} %refs_3_.11, ...), custom_call_target="tpu_custom_call" | custom-call | tf_op jit(solution)/shard_map/pallas_call | solution.py:109
  85.4 20.3 %collective-permute-done.4.refs_2_ = bf16[512,512]{1,0:T(8,128)(2,1)} collective-permute-done((bf16[512,512]{1,0:T(8,128)(2,1)}, bf16[512,512]{1,0:T(8,128)(2,1)}, u32[]{:S(2)}, u32[]{:S(2)}) %collective-permute-start.4) | collective-permute-done | bytes 524320 | tf_op jit(solution)/shard_map/ppermute | solution.py:42
  108.4 8.2 %shard_map.157 = (bf16[8,128,512]{2,1,0:T(8,128)(2,1)}, bf16[8,128,512]{2,1,0:T(8,128)(2,1)}, bf16[8,128,512]{2,1,0:T(8,128)(2,1)}, bf16[8,128,512]{2,1,0:T(8,128)(2,1)}, f32[8,128]{1,0:T(8,128)}) custom-call(s32[4]{0:T(128)} %get-tuple-element.113.idx_ref, f32[64,128,512]{2,1,0:T(8,128)} %refs_3_.11, f32[64,128,512]{2,1,0:T(8,128)} %refs_3_.11, ...), custom_call_target="tpu_custom_call" | custom-call | tf_op jit(solution)/shard_map/pallas_call | solution.py:109
  119.0 2.1 collective-permute-start.52
  122.5 7.4 %route.1 = (bf16[8,512,512]{2,1,0:T(8,128)(2,1)}, f32[512,1024]{1,0:T(8,128)}, f32[512,1]{1,0:T(8,128)}) custom-call(s32[1]{0:T(128)} %bitcast.8.me_ref, s32[8]{0:T(128)} %stack.64.from_ref.refs_0_, bf16[512,512]{1,0:T(8,128)(2,1)} %pack_tokens.1.refs_0_.refs_8_, bf16[512,512]{1,0:T(8,128)(2,1)} %collective-permute-done.3.refs_1_, ...), custom_call_target="tpu_custom_call" | custom-call | tf_op jit(solution)/shard_map/route/pallas_call | solution.py:167
  129.9 8.1 %shard_map.158 = (bf16[16,64,4096]{2,1,0:T(8,128)(2,1)}, bf16[16,64,4096]{2,1,0:T(8,128)(2,1)}, bf16[64,4096]{1,0:T(8,128)(2,1)}, bf16[64,4096]{1,0:T(8,128)(2,1)}, bf16[512,192]{1,0:T(8,128)(2,1)}) custom-call(s32[4]{0:T(128)} %get-tuple-element.114.refs_0_.refs_1_.blk_ref, bf16[8,512,512]{2,1,0:T(8,128)(2,1)} %get-tuple-element.62.refs_1_, ...), custom_call_target="tpu_custom_call" | custom-call | tf_op jit(solution)/shard_map/pallas_call | solution.py:347
  138.0 67.7 %collective-permute-done.49.refs_14_ = bf16[6,128,512]{2,1,0:T(8,128)(2,1)} collective-permute-done((bf16[6,128,512]{2,1,0:T(8,128)(2,1)}, bf16[6,128,512]{2,1,0:T(8,128)(2,1)}, u32[]{:S(2)}, u32[]{:S(2)}) %collective-permute-start.49) | collective-permute-done | bytes 786464 | tf_op jit(solution)/shard_map/ppermute | solution.py:29
  205.7 2.5 collective-permute-start.22
  211.0 6.2 %collective-permute-done.22.refs_3_.refs_5_ = bf16[512,192]{1,0:T(8,128)(2,1)} collective-permute-done((bf16[512,192]{1,0:T(8,128)(2,1)}, bf16[512,192]{1,0:T(8,128)(2,1)}, u32[]{:S(2)}, u32[]{:S(2)}) %collective-permute-start.22) | collective-permute-done | bytes 196640 | tf_op jit(solution)/shard_map/ppermute | solution.py:42
  217.2 9.0 %collective-permute-start.20 = (bf16[512,192]{1,0:T(8,128)(2,1)}, bf16[512,192]{1,0:T(8,128)(2,1)}, u32[]{:S(2)}, u32[]{:S(2)}) collective-permute-start(bf16[512,192]{1,0:T(8,128)(2,1)} %get-tuple-element.72.refs_0_.refs_2_), channel_id=1, source_target_pairs={{0,2},{1,3},{2,0},{3,1},{4,6},{5,7},{6,4},{7,5},{8,10},{9,11},{10,... | collective-permute-start | bytes 589832 | tf_op jit(solution)/shard_map/ppermute | solution.py:42
  226.2 4.6 collective-permute-done.21.refs_2_.refs_4_
  232.8 3.5 collective-permute-done.20.refs_1_.refs_3_
  238.7 130.7 %collective-permute-done.31.refs_6_ = bf16[2,6,64,1024]{3,2,1,0:T(8,128)(2,1)} collective-permute-done((bf16[2,6,64,1024]{3,2,1,0:T(8,128)(2,1)}, bf16[2,6,64,1024]{3,2,1,0:T(8,128)(2,1)}, u32[]{:S(2)}, u32[]{:S(2)}) %collective-permute-start.31) | collective-permute-done | bytes 1572896 | tf_op jit(solution)/shard_map/ppermute | solution.py:29
  369.9 10.1 %shard_map.159 = (bf16[16,64,4096]{2,1,0:T(8,128)(2,1)}, bf16[16,64,4096]{2,1,0:T(8,128)(2,1)}, bf16[512,384]{1,0:T(8,128)(2,1)}) custom-call(s32[4]{0:T(128)} %get-tuple-element.114.refs_0_.refs_1_.blk_ref, bf16[8,512,512]{2,1,0:T(8,128)(2,1)} %get-tuple-element.62.refs_1_, ...), custom_call_target="tpu_custom_call", output_to_operand_aliasing={{0}: (8, {}), {1}: (9, {})} | custom-call | tf_op jit(solution)/shard_map/pallas_call | solution.py:347
  385.0 10.7 %shard_map.160 = (bf16[16,64,4096]{2,1,0:T(8,128)(2,1)}, bf16[16,64,4096]{2,1,0:T(8,128)(2,1)}, bf16[512,512]{1,0:T(8,128)(2,1)}) custom-call(s32[4]{0:T(128)} %get-tuple-element.114.refs_0_.refs_1_.blk_ref, bf16[8,512,512]{2,1,0:T(8,128)(2,1)} %get-tuple-element.62.refs_1_, ...), custom_call_target="tpu_custom_call", output_to_operand_aliasing={{0}: (8, {}), {1}: (9, {})} | custom-call | tf_op jit(solution)/shard_map/pallas_call | solution.py:347
  397.1 14.4 %collective-permute-start.34 = (bf16[512,512]{1,0:T(8,128)(2,1)}, bf16[512,512]{1,0:T(8,128)(2,1)S(1)}, u32[]{:S(2)}, u32[]{:S(2)}) collective-permute-start(bf16[512,512]{1,0:T(8,128)(2,1)} %get-tuple-element.85.refs_2_), channel_id=1, source_target_pairs={{0,4},{1,5},{2,6},{3,7},{4,0},{5,1},{6,2},{7,3},{8,12},{9,13},{10,... | collective-permute-start | bytes 1572872 | tf_op jit(solution)/shard_map/ppermute | solution.py:42
  411.6 29.5 %collective-permute-done.41.refs_4_ = bf16[512,384]{1,0:T(8,128)(2,1)} collective-permute-done((bf16[512,384]{1,0:T(8,128)(2,1)}, bf16[512,384]{1,0:T(8,128)(2,1)}, u32[]{:S(2)}, u32[]{:S(2)}) %collective-permute-start.41) | collective-permute-done | bytes 393248 | tf_op jit(solution)/shard_map/ppermute | solution.py:42
  443.2 19.5 %collective-permute-done.34.refs_4_ = bf16[512,512]{1,0:T(8,128)(2,1)S(1)} collective-permute-done((bf16[512,512]{1,0:T(8,128)(2,1)}, bf16[512,512]{1,0:T(8,128)(2,1)S(1)}, u32[]{:S(2)}, u32[]{:S(2)}) %collective-permute-start.34) | collective-permute-done | bytes 524320 | tf_op jit(solution)/shard_map/ppermute | solution.py:42
  464.7 3.0 shard_map.163
  474.8 3.2 shared_down.1.refs_10_
  478.0 6.8 %shard_map.161 = (bf16[16,512,512]{2,1,0:T(8,128)(2,1)}, f32[512,512]{1,0:T(8,128)}) custom-call(s32[8]{0:T(128)} %stack.64.from_ref.refs_0_, s32[4]{0:T(128)} %get-tuple-element.114.refs_0_.refs_1_.blk_ref, bf16[512,384]{1,0:T(8,128)(2,1)} %get-tuple-element.86.refs_2_, bf16[512,384]{1,0:T(8,128)(2,1)} %collective-permute-done.40.refs_3_, ...), custom_call_target="tpu_custom_call" | custom-call | tf_op jit(solution)/shard_map/pallas_call | solution.py:491
  485.6 7.9 %shard_map.162 = (bf16[16,512,512]{2,1,0:T(8,128)(2,1)}, f32[512,512]{1,0:T(8,128)}) custom-call(s32[8]{0:T(128)} %stack.64.from_ref.refs_0_, s32[4]{0:T(128)} %get-tuple-element.114.refs_0_.refs_1_.blk_ref, bf16[512,512]{1,0:T(8,128)(2,1)} %get-tuple-element.85.refs_2_, bf16[512,512]{1,0:T(8,128)(2,1)} %copy-done.21, ...), custom_call_target="tpu_custom_call", output_to_operand_aliasing={{0}: (15, {})} | custom-call | tf_op jit(solution)/shard_map/pallas_call | solution.py:491
  495.4 4.3 shard_map.164
  504.0 3.0 finish.1
  (199 shorter events, 58.7 us)
Async XLA Ops:
  6.3 24.8 %collective-permute-start.17 = (bf16[2,64,1024]{2,1,0:T(8,128)(2,1)S(1)}, bf16[2,64,1024]{2,1,0:T(8,128)(2,1)S(1)}, u32[]{:S(2)}, u32[]{:S(2)}) collective-permute-start(bf16[2,64,1024]{2,1,0:T(8,128)(2,1)S(1)} %fusion.refs_8_), channel_id=1, source_target_pairs={{0,16},{8,24},{16,0},{24,8},{1,17},{9,25},{17,1},{25,9},{2,18},{10... | collective-permute-start | bytes 786440 | tf_op jit(solution)/shard_map/ppermute | solution.py:29
  8.3 25.8 %collective-permute-start.16 = (bf16[2,64,1024]{2,1,0:T(8,128)(2,1)S(1)}, bf16[2,64,1024]{2,1,0:T(8,128)(2,1)S(1)}, u32[]{:S(2)}, u32[]{:S(2)}) collective-permute-start(bf16[2,64,1024]{2,1,0:T(8,128)(2,1)S(1)} %fusion.refs_8_), channel_id=1, source_target_pairs={{0,8},{8,0},{16,24},{24,16},{1,9},{9,1},{17,25},{25,17},{2,10},{10... | collective-permute-start | bytes 786440 | tf_op jit(solution)/shard_map/ppermute | solution.py:29
  30.6 34.3 %collective-permute-start.13 = (bf16[2,2,64,1024]{3,2,1,0:T(8,128)(2,1)}, bf16[2,2,64,1024]{3,2,1,0:T(8,128)(2,1)S(1)}, u32[]{:S(2)}, u32[]{:S(2)}) collective-permute-start(bf16[2,2,64,1024]{3,2,1,0:T(8,128)(2,1)} %get-tuple-element.66), channel_id=1, source_target_pairs={{0,8},{8,0},{16,24},{24,16},{1,9},{9,1},{17,25},{25,17},{2,10},{10... | collective-permute-start | bytes 1572872 | tf_op jit(solution)/shard_map/ppermute | solution.py:29
  31.2 51.8 %collective-permute-start.14 = (bf16[2,2,64,1024]{3,2,1,0:T(8,128)(2,1)}, bf16[2,2,64,1024]{3,2,1,0:T(8,128)(2,1)S(1)}, u32[]{:S(2)}, u32[]{:S(2)}) collective-permute-start(bf16[2,2,64,1024]{3,2,1,0:T(8,128)(2,1)} %get-tuple-element.67), channel_id=1, source_target_pairs={{0,16},{8,24},{16,0},{24,8},{1,17},{9,25},{17,1},{25,9},{2,18},{10... | collective-permute-start | bytes 1572872 | tf_op jit(solution)/shard_map/ppermute | solution.py:29
  32.0 52.0 %collective-permute-start.15 = (bf16[2,2,64,1024]{3,2,1,0:T(8,128)(2,1)S(1)}, bf16[2,2,64,1024]{3,2,1,0:T(8,128)(2,1)S(1)}, u32[]{:S(2)}, u32[]{:S(2)}) collective-permute-start(bf16[2,2,64,1024]{3,2,1,0:T(8,128)(2,1)S(1)} %copy-done.40), channel_id=1, source_target_pairs={{0,24},{8,16},{16,8},{24,0},{1,25},{9,17},{17,9},{25,1},{2,26},{10... | collective-permute-start | bytes 1572872 | tf_op jit(solution)/shard_map/ppermute | solution.py:29
  34.2 50.7 %collective-permute-start.6 = (bf16[512,512]{1,0:T(8,128)(2,1)}, bf16[512,512]{1,0:T(8,128)(2,1)S(1)}, u32[]{:S(2)}, u32[]{:S(2)}) collective-permute-start(bf16[512,512]{1,0:T(8,128)(2,1)} %pack_tokens.1.refs_0_.refs_8_), channel_id=1, source_target_pairs={{0,1},{1,0},{2,3},{3,2},{4,5},{5,4},{6,7},{7,6},{8,9},{9,8},{10,11... | collective-permute-start | bytes 1572872 | tf_op jit(solution)/shard_map/ppermute | solution.py:48
  61.2 24.2 %collective-permute-start.5 = (bf16[512,512]{1,0:T(8,128)(2,1)}, bf16[512,512]{1,0:T(8,128)(2,1)}, u32[]{:S(2)}, u32[]{:S(2)}) collective-permute-start(bf16[512,512]{1,0:T(8,128)(2,1)} %pack_tokens.1.refs_0_.refs_8_), channel_id=1, source_target_pairs={{0,6},{1,7},{2,4},{3,5},{4,2},{5,3},{6,0},{7,1},{8,14},{9,15},{10,... | collective-permute-start | bytes 1572872 | tf_op jit(solution)/shard_map/ppermute | solution.py:42
  64.8 40.8 %collective-permute-start.4 = (bf16[512,512]{1,0:T(8,128)(2,1)}, bf16[512,512]{1,0:T(8,128)(2,1)}, u32[]{:S(2)}, u32[]{:S(2)}) collective-permute-start(bf16[512,512]{1,0:T(8,128)(2,1)} %pack_tokens.1.refs_0_.refs_8_), channel_id=1, source_target_pairs={{0,4},{1,5},{2,6},{3,7},{4,0},{5,1},{6,2},{7,3},{8,12},{9,13},{10,... | collective-permute-start | bytes 1572872 | tf_op jit(solution)/shard_map/ppermute | solution.py:42
  84.8 31.8 %collective-permute-start.48 = (bf16[6,128,512]{2,1,0:T(8,128)(2,1)}, bf16[6,128,512]{2,1,0:T(8,128)(2,1)S(1)}, u32[]{:S(2)}, u32[]{:S(2)}) collective-permute-start(bf16[6,128,512]{2,1,0:T(8,128)(2,1)} %get-tuple-element.89), channel_id=1, source_target_pairs={{0,16},{8,24},{16,0},{24,8},{1,17},{9,25},{17,1},{25,9},{2,18},{10... | collective-permute-start | bytes 2359304 | tf_op jit(solution)/shard_map/ppermute | solution.py:29
  85.4 32.8 %collective-permute-start.9 = (bf16[512,512]{1,0:T(8,128)(2,1)}, bf16[512,512]{1,0:T(8,128)(2,1)}, u32[]{:S(2)}, u32[]{:S(2)}) collective-permute-start(bf16[512,512]{1,0:T(8,128)(2,1)} %collective-permute-done.5.refs_3_), channel_id=1, source_target_pairs={{0,1},{1,0},{2,3},{3,2},{4,5},{5,4},{6,7},{7,6},{8,9},{9,8},{10,11... | collective-permute-start | bytes 1572872 | tf_op jit(solution)/shard_map/ppermute | solution.py:48
  107.1 130.5 %collective-permute-start.30 = (bf16[2,6,64,1024]{3,2,1,0:T(8,128)(2,1)}, bf16[2,6,64,1024]{3,2,1,0:T(8,128)(2,1)S(1)}, u32[]{:S(2)}, u32[]{:S(2)}) collective-permute-start(bf16[2,6,64,1024]{3,2,1,0:T(8,128)(2,1)} %get-tuple-element.78), channel_id=1, source_target_pairs={{0,8},{8,0},{16,24},{24,16},{1,9},{9,1},{17,25},{25,17},{2,10},{10... | collective-permute-start | bytes 4718600 | tf_op jit(solution)/shard_map/ppermute | solution.py:29
  117.5 88.1 %collective-permute-start.50 = (bf16[8,128,512]{2,1,0:T(8,128)(2,1)}, bf16[8,128,512]{2,1,0:T(8,128)(2,1)S(1)}, u32[]{:S(2)}, u32[]{:S(2)}) collective-permute-start(bf16[8,128,512]{2,1,0:T(8,128)(2,1)} %get-tuple-element.93), channel_id=1, source_target_pairs={{0,8},{8,0},{16,24},{24,16},{1,9},{9,1},{17,25},{25,17},{2,10},{10... | collective-permute-start | bytes 3145736 | tf_op jit(solution)/shard_map/ppermute | solution.py:29
  118.3 90.0 %collective-permute-start.51 = (bf16[8,128,512]{2,1,0:T(8,128)(2,1)}, bf16[8,128,512]{2,1,0:T(8,128)(2,1)}, u32[]{:S(2)}, u32[]{:S(2)}) collective-permute-start(bf16[8,128,512]{2,1,0:T(8,128)(2,1)} %get-tuple-element.94), channel_id=1, source_target_pairs={{0,16},{8,24},{16,0},{24,8},{1,17},{9,25},{17,1},{25,9},{2,18},{10... | collective-permute-start | bytes 3145736 | tf_op jit(solution)/shard_map/ppermute | solution.py:29
  119.0 89.3 %collective-permute-start.52 = (bf16[8,128,512]{2,1,0:T(8,128)(2,1)}, bf16[8,128,512]{2,1,0:T(8,128)(2,1)}, u32[]{:S(2)}, u32[]{:S(2)}) collective-permute-start(bf16[8,128,512]{2,1,0:T(8,128)(2,1)} %get-tuple-element.95), channel_id=1, source_target_pairs={{0,24},{8,16},{16,8},{24,0},{1,25},{9,17},{17,9},{25,1},{2,26},{10... | collective-permute-start | bytes 3145736 | tf_op jit(solution)/shard_map/ppermute | solution.py:29
  121.0 84.6 %collective-permute-start.49 = (bf16[6,128,512]{2,1,0:T(8,128)(2,1)}, bf16[6,128,512]{2,1,0:T(8,128)(2,1)}, u32[]{:S(2)}, u32[]{:S(2)}) collective-permute-start(bf16[6,128,512]{2,1,0:T(8,128)(2,1)} %get-tuple-element.90), channel_id=1, source_target_pairs={{0,24},{8,16},{16,8},{24,0},{1,25},{9,17},{17,9},{25,1},{2,26},{10... | collective-permute-start | bytes 2359304 | tf_op jit(solution)/shard_map/ppermute | solution.py:29
  208.3 173.2 %collective-permute-start.27 = (bf16[2,8,64,1024]{3,2,1,0:T(8,128)(2,1)}, bf16[2,8,64,1024]{3,2,1,0:T(8,128)(2,1)S(1)}, u32[]{:S(2)}, u32[]{:S(2)}) collective-permute-start(bf16[2,8,64,1024]{3,2,1,0:T(8,128)(2,1)} %get-tuple-element.74), channel_id=1, source_target_pairs={{0,8},{8,0},{16,24},{24,16},{1,9},{9,1},{17,25},{25,17},{2,10},{10... | collective-permute-start | bytes 6291464 | tf_op jit(solution)/shard_map/ppermute | solution.py:29
  209.3 172.7 %collective-permute-start.28 = (bf16[2,8,64,1024]{3,2,1,0:T(8,128)(2,1)}, bf16[2,8,64,1024]{3,2,1,0:T(8,128)(2,1)}, u32[]{:S(2)}, u32[]{:S(2)}) collective-permute-start(bf16[2,8,64,1024]{3,2,1,0:T(8,128)(2,1)} %get-tuple-element.75), channel_id=1, source_target_pairs={{0,16},{8,24},{16,0},{24,8},{1,17},{9,25},{17,1},{25,9},{2,18},{10... | collective-permute-start | bytes 6291464 | tf_op jit(solution)/shard_map/ppermute | solution.py:29
  230.8 152.9 %collective-permute-start.29 = (bf16[2,8,64,1024]{3,2,1,0:T(8,128)(2,1)}, bf16[2,8,64,1024]{3,2,1,0:T(8,128)(2,1)}, u32[]{:S(2)}, u32[]{:S(2)}) collective-permute-start(bf16[2,8,64,1024]{3,2,1,0:T(8,128)(2,1)} %get-tuple-element.76), channel_id=1, source_target_pairs={{0,24},{8,16},{16,8},{24,0},{1,25},{9,17},{17,9},{25,1},{2,26},{10... | collective-permute-start | bytes 6291464 | tf_op jit(solution)/shard_map/ppermute | solution.py:29
  236.3 133.1 %collective-permute-start.31 = (bf16[2,6,64,1024]{3,2,1,0:T(8,128)(2,1)}, bf16[2,6,64,1024]{3,2,1,0:T(8,128)(2,1)}, u32[]{:S(2)}, u32[]{:S(2)}) collective-permute-start(bf16[2,6,64,1024]{3,2,1,0:T(8,128)(2,1)} %get-tuple-element.79), channel_id=1, source_target_pairs={{0,16},{8,24},{16,0},{24,8},{1,17},{9,25},{17,1},{25,9},{2,18},{10... | collective-permute-start | bytes 4718600 | tf_op jit(solution)/shard_map/ppermute | solution.py:29
  237.6 131.8 %collective-permute-start.32 = (bf16[2,6,64,1024]{3,2,1,0:T(8,128)(2,1)}, bf16[2,6,64,1024]{3,2,1,0:T(8,128)(2,1)}, u32[]{:S(2)}, u32[]{:S(2)}) collective-permute-start(bf16[2,6,64,1024]{3,2,1,0:T(8,128)(2,1)} %get-tuple-element.80), channel_id=1, source_target_pairs={{0,24},{8,16},{16,8},{24,0},{1,25},{9,17},{17,9},{25,1},{2,26},{10... | collective-permute-start | bytes 4718600 | tf_op jit(solution)/shard_map/ppermute | solution.py:29
  382.0 59.1 %collective-permute-start.41 = (bf16[512,384]{1,0:T(8,128)(2,1)}, bf16[512,384]{1,0:T(8,128)(2,1)}, u32[]{:S(2)}, u32[]{:S(2)}) collective-permute-start(bf16[512,384]{1,0:T(8,128)(2,1)} %get-tuple-element.86.refs_2_), channel_id=1, source_target_pairs={{0,4},{1,5},{2,6},{3,7},{4,0},{5,1},{6,2},{7,3},{8,12},{9,13},{10,... | collective-permute-start | bytes 1179656 | tf_op jit(solution)/shard_map/ppermute | solution.py:42
  383.6 57.5 %collective-permute-start.40 = (bf16[512,384]{1,0:T(8,128)(2,1)}, bf16[512,384]{1,0:T(8,128)(2,1)}, u32[]{:S(2)}, u32[]{:S(2)}) collective-permute-start(bf16[512,384]{1,0:T(8,128)(2,1)} %get-tuple-element.86.refs_2_), channel_id=1, source_target_pairs={{0,2},{1,3},{2,0},{3,1},{4,6},{5,7},{6,4},{7,5},{8,10},{9,11},{10,... | collective-permute-start | bytes 1179656 | tf_op jit(solution)/shard_map/ppermute | solution.py:42
  395.7 46.0 %collective-permute-start.35 = (bf16[512,512]{1,0:T(8,128)(2,1)}, bf16[512,512]{1,0:T(8,128)(2,1)S(1)}, u32[]{:S(2)}, u32[]{:S(2)}) collective-permute-start(bf16[512,512]{1,0:T(8,128)(2,1)} %get-tuple-element.85.refs_2_), channel_id=1, source_target_pairs={{0,6},{1,7},{2,4},{3,5},{4,2},{5,3},{6,0},{7,1},{8,14},{9,15},{10,... | collective-permute-start | bytes 1572872 | tf_op jit(solution)/shard_map/ppermute | solution.py:42
  397.1 44.0 %collective-permute-start.46 = (bf16[512,384]{1,0:T(8,128)(2,1)S(1)}, bf16[512,384]{1,0:T(8,128)(2,1)S(1)}, u32[]{:S(2)}, u32[]{:S(2)}) collective-permute-start(bf16[512,384]{1,0:T(8,128)(2,1)S(1)} %collective-permute-done.42.refs_5_), channel_id=1, source_target_pairs={{0,1},{1,0},{2,3},{3,2},{4,5},{5,4},{6,7},{7,6},{8,9},{9,8},{10,11... | collective-permute-start | bytes 1179656 | tf_op jit(solution)/shard_map/ppermute | solution.py:48
  397.1 65.5 %collective-permute-start.34 = (bf16[512,512]{1,0:T(8,128)(2,1)}, bf16[512,512]{1,0:T(8,128)(2,1)S(1)}, u32[]{:S(2)}, u32[]{:S(2)}) collective-permute-start(bf16[512,512]{1,0:T(8,128)(2,1)} %get-tuple-element.85.refs_2_), channel_id=1, source_target_pairs={{0,4},{1,5},{2,6},{3,7},{4,0},{5,1},{6,2},{7,3},{8,12},{9,13},{10,... | collective-permute-start | bytes 1572872 | tf_op jit(solution)/shard_map/ppermute | solution.py:42
  441.1 27.8 %collective-permute-start.36 = (bf16[512,512]{1,0:T(8,128)(2,1)}, bf16[512,512]{1,0:T(8,128)(2,1)S(1)}, u32[]{:S(2)}, u32[]{:S(2)}) collective-permute-start(bf16[512,512]{1,0:T(8,128)(2,1)} %get-tuple-element.85.refs_2_), channel_id=1, source_target_pairs={{0,1},{1,0},{2,3},{3,2},{4,5},{5,4},{6,7},{7,6},{8,9},{9,8},{10,11... | collective-permute-start | bytes 1572872 | tf_op jit(solution)/shard_map/ppermute | solution.py:48
  441.7 28.5 %collective-permute-start.39 = (bf16[512,512]{1,0:T(8,128)(2,1)S(1)}, bf16[512,512]{1,0:T(8,128)(2,1)S(1)}, u32[]{:S(2)}, u32[]{:S(2)}) collective-permute-start(bf16[512,512]{1,0:T(8,128)(2,1)S(1)} %collective-permute-done.35.refs_5_), channel_id=1, source_target_pairs={{0,1},{1,0},{2,3},{3,2},{4,5},{5,4},{6,7},{7,6},{8,9},{9,8},{10,11... | collective-permute-start | bytes 1572872 | tf_op jit(solution)/shard_map/ppermute | solution.py:48
  443.0 24.7 %collective-permute-start.44 = (bf16[512,384]{1,0:T(8,128)(2,1)}, bf16[512,384]{1,0:T(8,128)(2,1)}, u32[]{:S(2)}, u32[]{:S(2)}) collective-permute-start(bf16[512,384]{1,0:T(8,128)(2,1)} %collective-permute-done.40.refs_3_), channel_id=1, source_target_pairs={{0,1},{1,0},{2,3},{3,2},{4,5},{5,4},{6,7},{7,6},{8,9},{9,8},{10,11... | collective-permute-start | bytes 1179656 | tf_op jit(solution)/shard_map/ppermute | solution.py:48
  467.8 25.8 %collective-permute-start.53 = (bf16[2,128,512]{2,1,0:T(8,128)(2,1)}, bf16[2,128,512]{2,1,0:T(8,128)(2,1)S(1)}, u32[]{:S(2)}, u32[]{:S(2)}) collective-permute-start(bf16[2,128,512]{2,1,0:T(8,128)(2,1)} %get-tuple-element.99), channel_id=1, source_target_pairs={{0,8},{8,0},{16,24},{24,16},{1,9},{9,1},{17,25},{25,17},{2,10},{10... | collective-permute-start | bytes 786440 | tf_op jit(solution)/shard_map/ppermute | solution.py:29
  468.9 25.7 %collective-permute-start.54 = (bf16[2,128,512]{2,1,0:T(8,128)(2,1)}, bf16[2,128,512]{2,1,0:T(8,128)(2,1)S(1)}, u32[]{:S(2)}, u32[]{:S(2)}) collective-permute-start(bf16[2,128,512]{2,1,0:T(8,128)(2,1)} %get-tuple-element.100), channel_id=1, source_target_pairs={{0,16},{8,24},{16,0},{24,8},{1,17},{9,25},{17,1},{25,9},{2,18},{10... | collective-permute-start | bytes 786440 | tf_op jit(solution)/shard_map/ppermute | solution.py:29
  470.2 24.4 %collective-permute-start.55 = (bf16[2,128,512]{2,1,0:T(8,128)(2,1)}, bf16[2,128,512]{2,1,0:T(8,128)(2,1)S(1)}, u32[]{:S(2)}, u32[]{:S(2)}) collective-permute-start(bf16[2,128,512]{2,1,0:T(8,128)(2,1)} %get-tuple-element.101), channel_id=1, source_target_pairs={{0,24},{8,16},{16,8},{24,0},{1,25},{9,17},{17,9},{25,1},{2,26},{10... | collective-permute-start | bytes 786440 | tf_op jit(solution)/shard_map/ppermute | solution.py:29
  473.0 29.2 %collective-permute-start.61 = (bf16[128,512]{1,0:T(8,128)(2,1)}, bf16[128,512]{1,0:T(8,128)(2,1)S(1)}, u32[]{:S(2)}, u32[]{:S(2)}) collective-permute-start(bf16[128,512]{1,0:T(8,128)(2,1)} %convert_element_type.23.refs_8_.refs_4_), channel_id=1, source_target_pairs={{0,24},{8,16},{16,8},{24,0},{1,25},{9,17},{17,9},{25,1},{2,26},{10... | collective-permute-start | bytes 393224 | tf_op jit(solution)/shard_map/ppermute | solution.py:29
  (71 other events, 1386.1 us)
